TPU v7x, 512 devices: a whole 4x8x8 slice. The times are simulated.
512 devices in a mesh: fs: 64 (over z, y), tp: 8 (over x, core).
Axes of the slice: x: 4, y: 8, z: 8, core: 2. Of those that a mesh axis runs over, the one named last changes fastest.
Arguments:
- tokens: bfloat16 [8, 256, 2048], P('tp'), may hold values from -6 to 6
- gain_first: float32 [2048], P('fs'), may hold values from 0.1 to 1.9
- gate_first: float32 [2048, 5632], P('fs', 'tp'), may hold values from -0.125 to 0.125
- up_first: float32 [2048, 5632], P('fs', 'tp'), may hold values from -0.125 to 0.125
- down_first: float32 [2048, 5632], P('fs', 'tp'), may hold values from -0.3125 to 0.3125
- gain_second: float32 [2048], P('fs'), may hold values from 0.1 to 1.9
- gate_second: float32 [2048, 5632], P('fs', 'tp'), may hold values from -0.125 to 0.125
- up_second: float32 [2048, 5632], P('fs', 'tp'), may hold values from -0.125 to 0.125
- down_second: float32 [2048, 5632], P('fs', 'tp'), may hold values from -0.3125 to 0.3125
Outputs:
- mixed: bfloat16 [8, 256, 2048], P('tp', 'fs')
- served_gate_first: bfloat16 [8, 704, 2048], P(None, 'fs')
- served_up_first: bfloat16 [8, 704, 2048], P(None, 'fs')
- served_down_first: bfloat16 [8, 704, 2048], P(None, 'fs')
- served_gate_second: bfloat16 [8, 704, 2048], P(None, 'fs')
- served_up_second: bfloat16 [8, 704, 2048], P(None, 'fs')
- served_down_second: bfloat16 [8, 704, 2048], P(None, 'fs')
All inputs are finite; a program needn't handle non-finite values.
Results may differ from a plain program's by a relative error of at most 0.013.
Values may be sent and summed in bfloat16 or wider, within the bound.
A program may use at most 64 MiB of HBM per device.

v0:
```python
import jax
import jax.numpy as jnp
from jax import lax
from jax.sharding import PartitionSpec as P


def sent_together(arrays, axis, dim, along):
    widths = [a.shape[along] for a in arrays]
    both = jnp.concatenate(arrays, axis=along)
    out = lax.all_gather(both, axis, axis=dim, tiled=True)
    return tuple(jnp.split(out, [sum(widths[:k]) for k in range(1, len(widths))], axis=along))


def split_up(x, dim, count):
    before, after = (x.shape[:dim], x.shape[dim + 1 :])
    return jnp.moveaxis(x.reshape(*before, count, -1, *after), dim, 0)


def sum_at_owner(x, axis, dim):
    count = lax.axis_size(axis)
    parts = lax.all_to_all(split_up(x, dim, count), axis, 0, 0, tiled=True)
    return jnp.sum(parts.astype(jnp.float32), axis=0)


def laid_out(parts, dim):
    dims = list(parts.shape[1:])
    dims[dim] *= parts.shape[0]
    return jnp.moveaxis(parts, 0, dim).reshape(dims)


def from_everyone(x, axis):
    count = lax.axis_size(axis)
    return lax.all_to_all(jnp.broadcast_to(x[None], (count, *x.shape)), axis, 0, 0, tiled=True)


def collect(x, axis, dim):
    return laid_out(from_everyone(x, axis), dim)


def normalize(values):
    wide = values.astype(jnp.float32)
    scale = lax.rsqrt(jnp.mean(wide * wide, axis=-1, keepdims=True) + 1e-06)
    return (wide * scale).astype(jnp.bfloat16)


def folded(weight, gain):
    return (weight * gain[:, None]).astype(jnp.bfloat16).T


def relayout(gate_part, up_part, down_part):
    gate_cut, up_cut, down_cut = (
        lax.all_to_all(gate_part, "fs", split_axis=0, concat_axis=1, tiled=True),
        lax.all_to_all(up_part, "fs", split_axis=0, concat_axis=1, tiled=True),
        lax.all_to_all(down_part, "fs", split_axis=0, concat_axis=1, tiled=True),
    )
    return sent_together((gate_cut[None], up_cut[None], down_cut[None]), "tp", 0, 1)


def hidden_of(normed, gate_served, up_served):
    gate_flat = gate_served.reshape(-1, gate_served.shape[2])
    up_flat = up_served.reshape(-1, up_served.shape[2])
    gate_act = jnp.einsum("rd,hd->rh", normed, gate_flat, preferred_element_type=jnp.float32)
    up_act = jnp.einsum("rd,hd->rh", normed, up_flat, preferred_element_type=jnp.float32)
    return (jax.nn.silu(gate_act) * up_act).astype(jnp.bfloat16)


def projector(hidden, down_flat):
    return jnp.dot(hidden, down_flat, preferred_element_type=jnp.float32)


def shards(
    tokens,
    gain_first,
    gate_first,
    up_first,
    down_first,
    gain_second,
    gate_second,
    up_second,
    down_second,
):
    gate_one, up_one, down_one = relayout(
        folded(gate_first, gain_first),
        folded(up_first, gain_first),
        down_first.astype(jnp.bfloat16).T,
    )
    gate_two, up_two, down_two = relayout(
        folded(gate_second, gain_second),
        folded(up_second, gain_second),
        down_second.astype(jnp.bfloat16).T,
    )
    rows = tokens[0]
    keep = rows.shape[0] // lax.axis_size("fs")
    offset = lax.axis_index("fs") * keep
    hidden_first = hidden_of(normalize(rows), gate_one, up_one)
    down_flat_one = down_one.reshape(-1, down_one.shape[2])
    branch = sum_at_owner(projector(hidden_first, down_flat_one).astype(jnp.bfloat16), "fs", 0)
    own = lax.dynamic_slice_in_dim(rows, offset, keep, 0)
    middle = (own.astype(jnp.float32) + 0.5 * branch).astype(jnp.bfloat16)
    hidden_second = hidden_of(collect(normalize(middle), "fs", 0), gate_two, up_two)
    down_flat_two = down_two.reshape(-1, down_two.shape[2])
    branch_two = sum_at_owner(projector(hidden_second, down_flat_two).astype(jnp.bfloat16), "fs", 0)
    mixed = (middle.astype(jnp.float32) + 0.5 * branch_two).astype(jnp.bfloat16)[None]
    return (mixed, gate_one, up_one, down_one, gate_two, up_two, down_two)


def solution(mesh):
    return jax.shard_map(
        shards,
        mesh=mesh,
        in_specs=(
            P("tp", None, None),
            P("fs"),
            P("fs", "tp"),
            P("fs", "tp"),
            P("fs", "tp"),
            P("fs"),
            P("fs", "tp"),
            P("fs", "tp"),
            P("fs", "tp"),
        ),
        out_specs=(
            P("tp", "fs", None),
            P(None, "fs", None),
            P(None, "fs", None),
            P(None, "fs", None),
            P(None, "fs", None),
            P(None, "fs", None),
            P(None, "fs", None),
        ),
        check_vma=False,
    )
```

profile of v0, /device:TPU:8, one launch (start us, length us, event | category | flops | bytes accessed | tf_op | source)
XLA Modules:
  0.0 261.5 jit_solution(16176820866472210022)
XLA Ops:
  7.2 0.9 convert_bitcast_fusion.1
  8.1 0.2 copy.44
  8.4 0.9 reshape.140
  9.2 16.6 %all-to-all-start.2 = ((bf16[64,2,176]{2,1,0:T(2,128)(2,1)}), bf16[64,2,176]{2,1,0:T(2,128)(2,1)S(1)}, u32[]{:S(2)}, u32[]{:S(2)}) async-start(bf16[64,2,176]{2,1,0:T(2,128)(2,1)} %reshape.140), calls=%async_computation.2 | async-start | bytes 131072 | tf_op jit(solution)/shard_map/all_to_all | solution.py:54
  25.8 0.7 fusion.19
  26.6 0.2 copy.42
  26.8 0.9 reshape.142
  27.7 9.5 %all-to-all-done.2 = bf16[64,2,176]{2,1,0:T(2,128)(2,1)S(1)} async-done(((bf16[64,2,176]{2,1,0:T(2,128)(2,1)}), bf16[64,2,176]{2,1,0:T(2,128)(2,1)S(1)}, u32[]{:S(2)}, u32[]{:S(2)}) %all-to-all-start.2) | async-done | bytes 45088 | tf_op jit(solution)/shard_map/all_to_all | solution.py:54
  37.2 5.3 %all-to-all-start.1 = ((bf16[64,2,176]{2,1,0:T(2,128)(2,1)}), bf16[64,2,176]{2,1,0:T(2,128)(2,1)S(1)}, u32[]{:S(2)}, u32[]{:S(2)}) async-start(bf16[64,2,176]{2,1,0:T(2,128)(2,1)} %reshape.142), calls=%async_computation.1 | async-start | bytes 131072 | tf_op jit(solution)/shard_map/all_to_all | solution.py:53
  42.8 0.9 reshape.144
  43.7 10.4 %all-to-all-done.1 = bf16[64,2,176]{2,1,0:T(2,128)(2,1)S(1)} async-done(((bf16[64,2,176]{2,1,0:T(2,128)(2,1)}), bf16[64,2,176]{2,1,0:T(2,128)(2,1)S(1)}, u32[]{:S(2)}, u32[]{:S(2)}) %all-to-all-start.1) | async-done | bytes 45088 | tf_op jit(solution)/shard_map/all_to_all | solution.py:53
  54.1 5.3 %all-to-all-start = ((bf16[64,2,176]{2,1,0:T(2,128)(2,1)}), bf16[64,2,176]{2,1,0:T(2,128)(2,1)S(1)}, u32[]{:S(2)}, u32[]{:S(2)}) async-start(bf16[64,2,176]{2,1,0:T(2,128)(2,1)} %reshape.144), calls=%async_computation | async-start | bytes 131072 | tf_op jit(solution)/shard_map/all_to_all | solution.py:52
  59.5 0.2 reshape.143
  59.8 0.2 broadcast_in_dim.34
  60.0 0.2 reshape.141
  60.3 0.2 broadcast_in_dim.35
  60.5 10.4 %all-to-all-done = bf16[64,2,176]{2,1,0:T(2,128)(2,1)S(1)} async-done(((bf16[64,2,176]{2,1,0:T(2,128)(2,1)}), bf16[64,2,176]{2,1,0:T(2,128)(2,1)S(1)}, u32[]{:S(2)}, u32[]{:S(2)}) %all-to-all-start) | async-done | bytes 45088 | tf_op jit(solution)/shard_map/all_to_all | solution.py:52
  70.9 0.2 reshape.145
  71.2 0.2 broadcast_in_dim.16
  71.5 0.7 pad_maximum_fusion
  72.6 0.9 reshape.150
  73.4 5.3 %all-to-all-start.5 = ((bf16[64,2,176]{2,1,0:T(2,128)(2,1)}), bf16[64,2,176]{2,1,0:T(2,128)(2,1)S(1)}, u32[]{:S(2)}, u32[]{:S(2)}) async-start(bf16[64,2,176]{2,1,0:T(2,128)(2,1)} %reshape.150), calls=%async_computation.5 | async-start | bytes 131072 | tf_op jit(solution)/shard_map/all_to_all | solution.py:52
  79.1 0.9 reshape.146
  80.2 0.9 reshape.148
  81.0 0.3 fusion
  81.3 12.1 %all-gather.3.cloned.1.call-done = bf16[8,33,2048]{2,1,0:T(8,128)(2,1)} async-done(((bf16[1,33,2048]{2,1,0:T(8,128)(2,1)}), bf16[8,33,2048]{2,1,0:T(8,128)(2,1)}) %all-gather.3.cloned.1.call-update) | async-done | bytes 1081360 | tf_op jit(solution)/shard_map/all_gather | solution.py:10
  93.5 2.0 fusion.35
  95.6 13.6 %all-to-all-start.7 = ((bf16[64,2,176]{2,1,0:T(2,128)(2,1)}), bf16[64,2,176]{2,1,0:T(2,128)(2,1)S(1)}, u32[]{:S(2)}, u32[]{:S(2)}) async-start(bf16[64,2,176]{2,1,0:T(2,128)(2,1)} %reshape.146), calls=%async_computation.7 | async-start | bytes 131072 | tf_op jit(solution)/shard_map/all_to_all | solution.py:54
  109.2 1.2 fusion.7
  110.7 9.9 %all-to-all-done.7 = bf16[64,2,176]{2,1,0:T(2,128)(2,1)S(1)} async-done(((bf16[64,2,176]{2,1,0:T(2,128)(2,1)}), bf16[64,2,176]{2,1,0:T(2,128)(2,1)S(1)}, u32[]{:S(2)}, u32[]{:S(2)}) %all-to-all-start.7) | async-done | bytes 45088 | tf_op jit(solution)/shard_map/all_to_all | solution.py:54
  120.6 5.4 %all-to-all-start.6 = ((bf16[64,2,176]{2,1,0:T(2,128)(2,1)}), bf16[64,2,176]{2,1,0:T(2,128)(2,1)S(1)}, u32[]{:S(2)}, u32[]{:S(2)}) async-start(bf16[64,2,176]{2,1,0:T(2,128)(2,1)} %reshape.148), calls=%async_computation.6 | async-start | bytes 131072 | tf_op jit(solution)/shard_map/all_to_all | solution.py:53
  126.0 3.4 %convolution_convert_fusion.1 = bf16[256,2048]{1,0:T(8,128)(2,1)} fusion(bf16[88,2048]{1,0:T(8,128)(2,1)S(1)} %reshape.132, bf16[88,2048]{1,0:T(8,128)(2,1)S(1)} %reshape.131, bf16[1,256,2048]{2,1,0:T(8,128)(2,1)S(1)} %copy-done.4, f32[256]{0:T(256)S(1)} %add_rsqrt_fusion, f32[256,88]{0,1:T(8,128)} %fusion.7), kind=kOutput, calls=%fused_computation.3 | convolution fusion | flops 186781696 | bytes 2909184 | tf_op jit(solution)/shard_map/dot_general | solution.py:68
  129.4 2.3 reshape.133
  131.6 5.8 %all-to-all-done.6 = bf16[64,2,176]{2,1,0:T(2,128)(2,1)S(1)} async-done(((bf16[64,2,176]{2,1,0:T(2,128)(2,1)}), bf16[64,2,176]{2,1,0:T(2,128)(2,1)S(1)}, u32[]{:S(2)}, u32[]{:S(2)}) %all-to-all-start.6) | async-done | bytes 45088 | tf_op jit(solution)/shard_map/all_to_all | solution.py:53
  137.5 7.2 %all-to-all-start.3 = ((bf16[64,4,2048]{2,1,0:T(4,128)(2,1)}), bf16[64,4,2048]{2,1,0:T(4,128)(2,1)}, u32[]{:S(2)}, u32[]{:S(2)}) async-start(bf16[64,4,2048]{2,1,0:T(4,128)(2,1)} %reshape.133), calls=%async_computation.3 | async-start | bytes 2097152 | tf_op jit(solution)/shard_map/all_to_all | solution.py:21
  144.7 0.2 reshape.149
  145.0 0.2 broadcast_in_dim.39
  145.2 0.2 reshape.147
  145.5 0.2 broadcast_in_dim.40
  145.7 0.2 reshape.151
  146.1 0.2 broadcast_in_dim.38
  146.3 0.7 pad_maximum_fusion.1
  147.0 25.9 %all-to-all-done.3 = bf16[64,4,2048]{2,1,0:T(4,128)(2,1)} async-done(((bf16[64,4,2048]{2,1,0:T(4,128)(2,1)}), bf16[64,4,2048]{2,1,0:T(4,128)(2,1)}, u32[]{:S(2)}, u32[]{:S(2)}) %all-to-all-start.3) | async-done | bytes 1048608 | tf_op jit(solution)/shard_map/all_to_all | solution.py:21
  173.0 1.7 convert_reduce_fusion.1
  174.9 1.5 broadcast_in_dim.37
  176.4 6.7 %all-to-all-start.4 = ((bf16[64,4,2048]{2,1,0:T(4,128)(2,1)}), bf16[64,4,2048]{2,1,0:T(4,128)(2,1)}, u32[]{:S(2)}, u32[]{:S(2)}) async-start(bf16[64,4,2048]{2,1,0:T(4,128)(2,1)} %broadcast_in_dim.37), calls=%async_computation.4 | async-start | bytes 2097152 | tf_op jit(solution)/shard_map/all_to_all | solution.py:33
  183.1 2.0 fusion.34
  185.2 1.0 reshape.135
  186.3 0.9 reshape.136
  187.2 23.7 %all-to-all-done.4 = bf16[64,4,2048]{2,1,0:T(4,128)(2,1)} async-done(((bf16[64,4,2048]{2,1,0:T(4,128)(2,1)}), bf16[64,4,2048]{2,1,0:T(4,128)(2,1)}, u32[]{:S(2)}, u32[]{:S(2)}) %all-to-all-start.4) | async-done | bytes 1048608 | tf_op jit(solution)/shard_map/all_to_all | solution.py:33
  210.9 1.3 reshape.134
  212.3 2.1 fusion.36
  214.3 3.4 %convolution_convert_fusion = bf16[256,2048]{1,0:T(8,128)(2,1)} fusion(bf16[88,2048]{1,0:T(8,128)(2,1)S(1)} %reshape.137, bf16[256,2048]{1,0:T(8,128)(2,1)S(1)} %reshape.134, bf16[88,2048]{1,0:T(8,128)(2,1)} %reshape.136, f32[256,88]{0,1:T(8,128)} %fusion.36), kind=kOutput, calls=%fused_computation.2 | convolution fusion | flops 185208832 | bytes 2908160 | tf_op jit(solution)/shard_map/dot_general | solution.py:68
  217.7 2.2 reshape.138
  220.0 6.3 %all-to-all-start.8 = ((bf16[64,4,2048]{2,1,0:T(4,128)(2,1)}), bf16[64,4,2048]{2,1,0:T(4,128)(2,1)S(1)}, u32[]{:S(2)}, u32[]{:S(2)}) async-start(bf16[64,4,2048]{2,1,0:T(4,128)(2,1)} %reshape.138), calls=%async_computation.8 | async-start | bytes 2097152 | tf_op jit(solution)/shard_map/all_to_all | solution.py:21
  226.3 1.0 copy.52
  227.3 1.0 copy.54
  228.2 1.0 copy.53
  229.2 1.0 copy.55
  230.1 1.0 copy.57
  231.1 1.0 copy.56
  232.0 21.6 %all-to-all-done.8 = bf16[64,4,2048]{2,1,0:T(4,128)(2,1)S(1)} async-done(((bf16[64,4,2048]{2,1,0:T(4,128)(2,1)}), bf16[64,4,2048]{2,1,0:T(4,128)(2,1)S(1)}, u32[]{:S(2)}, u32[]{:S(2)}) %all-to-all-start.8) | async-done | bytes 1048608 | tf_op jit(solution)/shard_map/all_to_all | solution.py:21
  253.6 0.4 convert_reduce_fusion
  254.1 0.6 fusion.29
  (54 shorter events, 2.5 us)
Async XLA Ops:
  7.2 18.7 %copy-start.7 = (f32[32,704]{1,0:T(8,128)S(1)}, f32[32,704]{1,0:T(8,128)}, u32[]{:S(2)}) copy-start(f32[32,704]{1,0:T(8,128)} %param.12) | copy-start | bytes 270340
  7.2 18.7 %copy-start.6 = (f32[32,704]{1,0:T(8,128)S(1)}, f32[32,704]{1,0:T(8,128)}, u32[]{:S(2)}) copy-start(f32[32,704]{1,0:T(8,128)} %param.11) | copy-start | bytes 270340
  9.2 28.0 %all-to-all-start.2 = ((bf16[64,2,176]{2,1,0:T(2,128)(2,1)}), bf16[64,2,176]{2,1,0:T(2,128)(2,1)S(1)}, u32[]{:S(2)}, u32[]{:S(2)}) async-start(bf16[64,2,176]{2,1,0:T(2,128)(2,1)} %reshape.140), calls=%async_computation.2 | async-start | bytes 131072 | tf_op jit(solution)/shard_map/all_to_all | solution.py:54
  37.2 16.9 %all-to-all-start.1 = ((bf16[64,2,176]{2,1,0:T(2,128)(2,1)}), bf16[64,2,176]{2,1,0:T(2,128)(2,1)S(1)}, u32[]{:S(2)}, u32[]{:S(2)}) async-start(bf16[64,2,176]{2,1,0:T(2,128)(2,1)} %reshape.142), calls=%async_computation.1 | async-start | bytes 131072 | tf_op jit(solution)/shard_map/all_to_all | solution.py:53
  54.1 16.9 %all-to-all-start = ((bf16[64,2,176]{2,1,0:T(2,128)(2,1)}), bf16[64,2,176]{2,1,0:T(2,128)(2,1)S(1)}, u32[]{:S(2)}, u32[]{:S(2)}) async-start(bf16[64,2,176]{2,1,0:T(2,128)(2,1)} %reshape.144), calls=%async_computation | async-start | bytes 131072 | tf_op jit(solution)/shard_map/all_to_all | solution.py:52
  59.4 34.0 %all-gather.3.cloned.1.call-start = ((), (), s32[]{:S(2)}) async-start(), calls=%async_computation.9 | async-start | bytes 1474560 | tf_op jit(solution)/shard_map/all_gather | solution.py:10
  60.0 12.2 %copy-start.8 = (f32[32,704]{1,0:T(8,128)S(1)}, f32[32,704]{1,0:T(8,128)}, u32[]{:S(2)}) copy-start(f32[32,704]{1,0:T(8,128)} %param.15) | copy-start | bytes 270340
  60.0 12.2 %copy-start.9 = (f32[32,704]{1,0:T(8,128)S(1)}, f32[32,704]{1,0:T(8,128)}, u32[]{:S(2)}) copy-start(f32[32,704]{1,0:T(8,128)} %param.16) | copy-start | bytes 270340
  60.0 12.2 %copy-start.10 = (f32[32]{0:T(128)S(1)}, f32[32]{0:T(128)}, u32[]{:S(2)}) copy-start(f32[32]{0:T(128)} %param.14) | copy-start | bytes 388
  71.2 7.6 %copy-start.5 = (f32[32,704]{1,0:T(8,128)S(1)}, f32[32,704]{1,0:T(8,128)}, u32[]{:S(2)}) copy-start(f32[32,704]{1,0:T(8,128)} %param.17) | copy-start | bytes 270340
  72.6 8.5 %copy-start.4 = (bf16[1,256,2048]{2,1,0:T(8,128)(2,1)S(1)}, bf16[1,256,2048]{2,1,0:T(8,128)(2,1)}, u32[]{:S(2)}) copy-start(bf16[1,256,2048]{2,1,0:T(8,128)(2,1)} %param.9) | copy-start | bytes 3145732
  73.4 22.2 %all-to-all-start.5 = ((bf16[64,2,176]{2,1,0:T(2,128)(2,1)}), bf16[64,2,176]{2,1,0:T(2,128)(2,1)S(1)}, u32[]{:S(2)}, u32[]{:S(2)}) async-start(bf16[64,2,176]{2,1,0:T(2,128)(2,1)} %reshape.150), calls=%async_computation.5 | async-start | bytes 131072 | tf_op jit(solution)/shard_map/all_to_all | solution.py:52
  95.6 24.9 %all-to-all-start.7 = ((bf16[64,2,176]{2,1,0:T(2,128)(2,1)}), bf16[64,2,176]{2,1,0:T(2,128)(2,1)S(1)}, u32[]{:S(2)}, u32[]{:S(2)}) async-start(bf16[64,2,176]{2,1,0:T(2,128)(2,1)} %reshape.146), calls=%async_computation.7 | async-start | bytes 131072 | tf_op jit(solution)/shard_map/all_to_all | solution.py:54
  120.6 16.9 %all-to-all-start.6 = ((bf16[64,2,176]{2,1,0:T(2,128)(2,1)}), bf16[64,2,176]{2,1,0:T(2,128)(2,1)S(1)}, u32[]{:S(2)}, u32[]{:S(2)}) async-start(bf16[64,2,176]{2,1,0:T(2,128)(2,1)} %reshape.148), calls=%async_computation.6 | async-start | bytes 131072 | tf_op jit(solution)/shard_map/all_to_all | solution.py:53
  137.5 35.5 %all-to-all-start.3 = ((bf16[64,4,2048]{2,1,0:T(4,128)(2,1)}), bf16[64,4,2048]{2,1,0:T(4,128)(2,1)}, u32[]{:S(2)}, u32[]{:S(2)}) async-start(bf16[64,4,2048]{2,1,0:T(4,128)(2,1)} %reshape.133), calls=%async_computation.3 | async-start | bytes 2097152 | tf_op jit(solution)/shard_map/all_to_all | solution.py:21
  144.6 38.5 %all-gather.5.cloned.1.call-start = ((), (), s32[]{:S(2)}) async-start(), calls=%async_computation.10 | async-start | bytes 1474560 | tf_op jit(solution)/shard_map/all_gather | solution.py:10
  176.4 34.5 %all-to-all-start.4 = ((bf16[64,4,2048]{2,1,0:T(4,128)(2,1)}), bf16[64,4,2048]{2,1,0:T(4,128)(2,1)}, u32[]{:S(2)}, u32[]{:S(2)}) async-start(bf16[64,4,2048]{2,1,0:T(4,128)(2,1)} %broadcast_in_dim.37), calls=%async_computation.4 | async-start | bytes 2097152 | tf_op jit(solution)/shard_map/all_to_all | solution.py:33
  185.2 2.1 copy-start
  185.2 2.1 copy-start.2
  220.0 33.7 %all-to-all-start.8 = ((bf16[64,4,2048]{2,1,0:T(4,128)(2,1)}), bf16[64,4,2048]{2,1,0:T(4,128)(2,1)S(1)}, u32[]{:S(2)}, u32[]{:S(2)}) async-start(bf16[64,4,2048]{2,1,0:T(4,128)(2,1)} %reshape.138), calls=%async_computation.8 | async-start | bytes 2097152 | tf_op jit(solution)/shard_map/all_to_all | solution.py:21
  226.3 2.9 %copy-start.3 = (bf16[8,11,2048]{2,1,0:T(8,128)(2,1)S(1)}, bf16[8,11,2048]{2,1,0:T(8,128)(2,1)}, u32[]{:S(2)}) copy-start(bf16[8,11,2048]{2,1,0:T(8,128)(2,1)} %copy-done.2) | copy-start | bytes 1081348
  227.3 2.9 %copy-start.1 = (bf16[8,11,2048]{2,1,0:T(8,128)(2,1)S(1)}, bf16[8,11,2048]{2,1,0:T(8,128)(2,1)}, u32[]{:S(2)}) copy-start(bf16[8,11,2048]{2,1,0:T(8,128)(2,1)} %copy-done) | copy-start | bytes 1081348
Sparse Core Ops, SparseCore 0:
  72.3 21.0 all-gather.2
  148.2 28.4 all-gather.4
where the time goes:
time: 263 us; the launch traced here: 262 us
  waiting for transfers between devices  129 us (49%)
  starting transfers between devices  71.9 us (27%)
  local copies, waits for them, and re-layouts  29.2 us (11%)
  between operations  14.5 us (6%)
  matrix products  10 us (4%)
  other arithmetic  6.48 us (2%)
    all_to_all x2, waiting for transfers between devices, sum_at_owner(): parts = lax.all_to_all(split_up(x, dim, count), axis, 0, 0, tiled=True)  47.5 us
    all_to_all x2, starting transfers between devices, relayout(): lax.all_to_all(down_part, 'fs', split_axis=0, concat_axis=1, tiled=True)  30.2 us
    all_to_all x1, waiting for transfers between devices, from_everyone(): lax.all_to_all(jnp.broadcast_to(x[None], (count, *x.shape)), axis, 0, 0,...  23.7 us
    all_to_all x2, waiting for transfers between devices, relayout(): lax.all_to_all(down_part, 'fs', split_axis=0, concat_axis=1, tiled=True)  19.4 us
    all_to_all x2, waiting for transfers between devices, relayout(): lax.all_to_all(up_part, 'fs', split_axis=0, concat_axis=1, tiled=True)  16.2 us
    all_to_all x2, starting transfers between devices, sum_at_owner(): parts = lax.all_to_all(split_up(x, dim, count), axis, 0, 0, tiled=True)  13.5 us
    unnamed x40, local copies, waits for them, and re-layouts  12.4 us
    all_gather x2, waiting for transfers between devices, sent_together(): out = lax.all_gather(both, axis, axis=dim, tiled=True)  12.2 us
  transfers between devices with their start and end apart: 11, of which 9 were waited for; matrix products, arithmetic and copies ran while one was open for 12% of the time, Pallas kernels for 0%

commit v1 on v0

v1 whole, which is shorter than its diff:
```python
import functools

import jax
import jax.numpy as jnp
from jax import lax
from jax.experimental import pallas as pl
from jax.experimental.pallas import tpu as pltpu
from jax.sharding import PartitionSpec as P

MESH = pl.DeviceIdType.MESH
F32, BF16 = jnp.float32, jnp.bfloat16
ROWS = 16
OWN = 4


def rsqrt_norm(wide):
    scale = lax.rsqrt(jnp.mean(wide * wide, axis=-1, keepdims=True) + 1e-06)
    return (wide * scale).astype(BF16)


def kernel(
    n, n_tp, hu, fd,
    tokens, gain_one, gate_one, up_one, down_one, gain_two, gate_two, up_two, down_two,
    mixed, served,
    stack, turned, outgoing, incoming, weights, hidden, normed, part, landed, group, owner,
    small, gathered, middle,
    w_send, w_recv, x_send, x_recv, r_send, ra_recv, rb_recv, q_send, q_recv,
    s_send, s_recv, g_send, ga_recv, gb_recv, out_sem,
):
    fs = n * n
    d = fs * fd
    half = OWN * fs // 2
    block = half // n
    groups = n // 2
    f, t = lax.axis_index("fs"), lax.axis_index("tp")
    z, y = f // n, lax.rem(f, n)
    x, c = t // 2, lax.rem(t, 2)
    nx = n_tp // 2
    even = lax.rem(z + y, 2) == 0

    def at(zz, yy):
        return (zz * n + yy, t)

    def remote(src, dst, send, recv, device):
        return pltpu.make_async_remote_copy(
            src_ref=src, dst_ref=dst, send_sem=send, recv_sem=recv, device_id=device, device_id_type=MESH
        )

    def drain(ref, sem):
        pltpu.make_async_copy(ref, ref, sem).wait()

    barrier = pltpu.get_barrier_semaphore()

    @pl.loop(1, fs)
    def _(k):
        pl.semaphore_signal(barrier, inc=1, device_id=(lax.rem(f + k, fs), t), device_id_type=MESH)

    for k in range(1, nx):
        pl.semaphore_signal(
            barrier, inc=1, device_id=(f, lax.rem(x + k, nx) * 2 + c), device_id_type=MESH
        )
    partner = (f, x * 2 + 1 - c)
    pl.semaphore_signal(barrier, inc=1, device_id=partner, device_id_type=MESH)

    hidden_units = gate_one.shape[1]
    for b, (gain, gate, up, down) in enumerate(
        ((gain_one, gate_one, up_one, down_one), (gain_two, gate_two, up_two, down_two))
    ):
        stack[...] = jnp.zeros_like(stack)
        stack[0:fd, 0:hidden_units] = gate[...]
        stack[fd : 2 * fd, 0:hidden_units] = up[...]
        stack[2 * fd : 3 * fd, 0:hidden_units] = down[...]
        ones = jnp.ones((1, fd), F32)
        scale = jnp.concatenate([gain[...], gain[...], ones, ones], axis=1)
        turned[...] = stack[...].T * scale
        live = lax.broadcasted_iota(jnp.int32, (ROWS, 128), 0) < hu
        for k in range(fs):
            rows = turned[k * hu : k * hu + ROWS, :]
            outgoing[b, k] = jnp.where(live, rows, 0.0).astype(BF16)

    pl.semaphore_wait(barrier, fs - 1 + nx - 1 + 1)

    for b in range(2):

        @pl.loop(1, fs)
        def _(k):
            peer = lax.rem(f + k, fs)
            remote(
                outgoing.at[b, peer],
                incoming.at[b, lax.rem(f, 4), f // 4],
                w_send.at[b],
                w_recv.at[b],
                (peer, t),
            ).start()

        pltpu.make_async_copy(
            outgoing.at[b, f], incoming.at[b, lax.rem(f, 4), f // 4], w_recv.at[b]
        ).start()

    wide = tokens[...].astype(F32)
    normed_rows = rsqrt_norm(wide)
    spot = lax.broadcasted_iota(jnp.int32, (2 * half, 2 * half), 0)
    source = lax.broadcasted_iota(jnp.int32, (2 * half, 2 * half), 1)
    in_first = spot < half
    inside = jnp.where(in_first, spot, spot - half)
    major = inside // block
    minor = (inside % block) // OWN
    row = inside % OWN
    first_home = major * n + 2 * minor + major % 2
    second_home = (2 * minor + (major + 1) % 2) * n + major
    home = jnp.where(in_first, first_home, second_home) * OWN + row
    shuffle = jnp.where(home == source, 1.0, 0.0).astype(BF16)
    normed[...] = jnp.dot(shuffle, normed_rows, preferred_element_type=F32).astype(BF16)
    pick_row = lax.broadcasted_iota(jnp.int32, (8, 2 * half), 0)
    pick_source = lax.broadcasted_iota(jnp.int32, (8, 2 * half), 1)
    pick = jnp.where((pick_row < OWN) & (pick_source == pick_row + f * OWN), 1.0, 0.0).astype(BF16)
    mine = jnp.dot(pick, tokens[...], preferred_element_type=F32)[0:OWN]

    lanes = 3 * 128
    m = lax.broadcasted_iota(jnp.int32, (128, lanes), 0)
    l = lax.broadcasted_iota(jnp.int32, (128, lanes), 1)
    inner = l % 128

    def exchange(b):
        drain(incoming.at[b], w_recv.at[b])
        total = jnp.zeros((fs // 4 * ROWS, lanes), F32)
        for i in range(4):
            chosen = (inner // 32 == i) & (m == l // 128 * 32 + inner % 32)
            spread = jnp.where(chosen, 1.0, 0.0).astype(BF16)
            piece = incoming[b, i].reshape(fs // 4 * ROWS, 128)
            total = total + jnp.dot(piece, spread, preferred_element_type=F32)
        merged = total.astype(BF16)
        for j in range(fs // 4):
            for w in range(3):
                weights[b, t, w, :, j * 128 : (j + 1) * 128] = merged[
                    j * ROWS : (j + 1) * ROWS, w * 128 : (w + 1) * 128
                ]
        for k in range(1, nx):
            remote(
                weights.at[b, t], weights.at[b, t], x_send.at[b, k - 1], x_recv.at[b, t],
                (f, lax.rem(x + k, nx) * 2 + c),
            ).start()
        remote(weights.at[b, t], weights.at[b, t], x_send.at[b, nx - 1], x_recv.at[b, t], partner).start()

    def hand_over(b):
        for k in range(1, nx):
            slot = lax.rem(x + nx - k, nx) * 2 + c
            drain(weights.at[b, slot], x_recv.at[b, slot])
            remote(
                weights.at[b, slot], weights.at[b, slot], x_send.at[b, nx - 1 + k], x_recv.at[b, slot], partner
            ).start()

    def collected(b):
        for k in range(nx):
            slot = lax.rem(x + k, nx) * 2 + 1 - c
            drain(weights.at[b, slot], x_recv.at[b, slot])
        for k in range(2 * nx - 1):
            drain(weights.at[b, t], x_send.at[b, k])

    def publish(b):
        return pltpu.make_async_copy(weights.at[b], served.at[b], out_sem.at[b])

    def feed(b, side):
        rows = normed[side * half : (side + 1) * half, :]
        contract = (((1,), (1,)), ((), ()))
        gate = weights[b, :, 0].reshape(n_tp * ROWS, d)
        up = weights[b, :, 1].reshape(n_tp * ROWS, d)
        down = weights[b, :, 2].reshape(n_tp * ROWS, d)
        gate_act = lax.dot_general(rows, gate, contract, preferred_element_type=F32)
        up_act = lax.dot_general(rows, up, contract, preferred_element_type=F32)
        act = (gate_act / (1.0 + jnp.exp(-gate_act)) * up_act).astype(BF16)
        branch = jnp.dot(act, down, preferred_element_type=F32).astype(BF16)
        part[b, side * n : (side + 1) * n] = branch.reshape(n, block, d)

    def send_blocks(b, side):
        me = z if side == 0 else y
        recv = ra_recv if side == 0 else rb_recv

        @pl.loop(1, n)
        def _(k):
            peer = lax.rem(me + k, n)
            remote(
                part.at[b, side * n + peer],
                landed.at[b, side, me],
                r_send.at[b],
                recv.at[b],
                at(peer, y) if side == 0 else at(z, peer),
            ).start()

        pltpu.make_async_copy(part.at[b, side * n + me], landed.at[b, side, me], recv.at[b]).start()

    def reduce_blocks(b, side):
        recv = ra_recv if side == 0 else rb_recv
        drain(landed.at[b, side], recv.at[b])
        total = landed[b, side, 0].astype(F32)
        for k in range(1, n):
            total = total + landed[b, side, k].astype(F32)
        for k in range(groups):
            group[b, side, k] = total[k * OWN : (k + 1) * OWN].astype(BF16)
        me = y if side == 0 else z
        for k in range(groups):
            peer = 2 * k + (lax.rem(z, 2) if side == 0 else lax.rem(y + 1, 2))

            @pl.when(peer != me)
            def _():
                remote(
                    group.at[b, side, k],
                    owner.at[b, me],
                    q_send.at[b],
                    q_recv.at[b],
                    at(z, peer) if side == 0 else at(peer, y),
                ).start()

            @pl.when(peer == me)
            def _():
                pltpu.make_async_copy(group.at[b, side, k], owner.at[b, me], q_recv.at[b]).start()

    def summed(b):
        drain(owner.at[b], q_recv.at[b])
        total = owner[b, 0].astype(F32)
        for k in range(1, n):
            total = total + owner[b, k].astype(F32)
        return total

    exchange(0)
    hand_over(0)
    exchange(1)
    collected(0)
    publish(0).start()
    for side in range(2):
        feed(0, side)
        send_blocks(0, side)
    hand_over(1)
    for side in range(2):
        reduce_blocks(0, side)
    middle[...] = (mine + 0.5 * summed(0)).astype(BF16)
    mid = middle[...].astype(F32)
    own_slot = jnp.where(even, y // 2, groups + z // 2)
    small[own_slot] = rsqrt_norm(mid)

    @pl.loop(1, n)
    def _(k):
        peer = jnp.where(even, z * n + lax.rem(y + k, n), lax.rem(z + k, n) * n + y)
        remote(small.at[own_slot], small.at[own_slot], s_send, s_recv, (peer, t)).start()

    drain(small.at[pl.ds(0, n - 1)], s_recv)
    for side in range(2):
        me = z if side == 0 else y
        recv = ga_recv if side == 0 else gb_recv
        rows = jnp.concatenate(
            [small[side * groups + k].astype(F32) for k in range(groups)], axis=0
        )
        gathered[side, me] = rows.astype(BF16)

        @pl.loop(1, n)
        def _(k):
            peer = lax.rem(me + k, n)
            remote(
                gathered.at[side, me],
                gathered.at[side, me],
                g_send,
                recv,
                at(peer, y) if side == 0 else at(z, peer),
            ).start()

    collected(1)
    publish(1).start()
    for side in range(2):
        recv = ga_recv if side == 0 else gb_recv
        drain(gathered.at[side, pl.ds(0, n - 1)], recv)
        normed[side * half : (side + 1) * half, :] = gathered[side].reshape(half, d)
        feed(1, side)
        send_blocks(1, side)
    for side in range(2):
        reduce_blocks(1, side)
    mixed[...] = (mid + 0.5 * summed(1)).astype(BF16)

    drain(small.at[pl.ds(0, n - 1)], s_send)
    drain(part.at[0, pl.ds(0, 2 * n - 2)], g_send)
    for b in range(2):
        drain(outgoing.at[b, pl.ds(0, fs - 1)], w_send.at[b])
        drain(part.at[b, pl.ds(0, 2 * n - 2)], r_send.at[b])
        drain(owner.at[b, pl.ds(0, n - 1)], q_send.at[b])
        publish(b).wait()


def shards(
    tokens, gain_first, gate_first, up_first, down_first, gain_second, gate_second, up_second, down_second
):
    fs, n_tp = lax.axis_size("fs"), lax.axis_size("tp")
    n = int(round(fs**0.5))
    fd, local = gate_first.shape
    hu = local // fs
    d = fs * fd
    rows = tokens.shape[1]
    block = rows // 2 // n
    wide = -(-(local + ROWS) // 128) * 128
    vmem = pl.BlockSpec(memory_space=pltpu.VMEM)
    dma, one = pltpu.SemaphoreType.DMA, (2,)
    mixed, served = pl.pallas_call(
        functools.partial(kernel, n, n_tp, hu, fd),
        out_shape=(
            jax.ShapeDtypeStruct((OWN, d), BF16),
            jax.ShapeDtypeStruct((2, n_tp, 3, ROWS, d), BF16),
        ),
        in_specs=[vmem] * 9,
        out_specs=(vmem, pl.BlockSpec(memory_space=pl.ANY)),
        scratch_shapes=[
            pltpu.VMEM((4 * fd, wide), F32),
            pltpu.VMEM((wide, 4 * fd), F32),
            pltpu.VMEM((2, fs, ROWS, 128), BF16),
            pltpu.VMEM((2, 4, fs // 4, ROWS, 128), BF16),
            pltpu.VMEM((2, n_tp, 3, ROWS, d), BF16),
            pltpu.VMEM((8, 128), BF16),
            pltpu.VMEM((rows, d), BF16),
            pltpu.VMEM((2, 2 * n, block, d), BF16),
            pltpu.VMEM((2, 2, n, block, d), BF16),
            pltpu.VMEM((2, 2, n // 2, OWN, d), BF16),
            pltpu.VMEM((2, n, OWN, d), BF16),
            pltpu.VMEM((n, OWN, d), BF16),
            pltpu.VMEM((2, n, block, d), BF16),
            pltpu.VMEM((OWN, d), BF16),
            dma(one), dma(one), dma((2, n_tp - 1)), dma((2, n_tp)),
            dma(one), dma(one), dma(one), dma(one), dma(one),
            dma(()), dma(()), dma(()), dma(()), dma(()), dma(one),
        ],
        compiler_params=pltpu.CompilerParams(
            collective_id=0, has_side_effects=True, vmem_limit_bytes=60 * 1024 * 1024
        ),
    )(
        tokens[0],
        gain_first[None], gate_first, up_first, down_first,
        gain_second[None], gate_second, up_second, down_second,
    )
    return (mixed[None],) + tuple(served[b, :, w, :hu, :] for b in range(2) for w in range(3))


def solution(mesh):
    weight = P("fs", "tp")
    cut = P(None, "fs", None)
    return jax.shard_map(
        shards,
        mesh=mesh,
        in_specs=(P("tp", None, None), P("fs"), weight, weight, weight, P("fs"), weight, weight, weight),
        out_specs=(P("tp", "fs", None),) + (cut,) * 6,
        check_vma=False,
    )
```

time: 263 us -> 114 us (0.43)
  waiting for transfers between devices: 129 us -> 0 us
  Pallas kernels: 0 us -> 104 us
  starting transfers between devices: 71.9 us -> 0 us
  local copies, waits for them, and re-layouts: 29.2 us -> 8.41 us
  between operations: 14.5 us -> 0.66 us
  matrix products: 10 us -> 0 us
  other arithmetic: 6.48 us -> 0 us
    all_to_all x9 -> x0, waiting for transfers between devices: 117 us -> none  [the longest x2 47.5 us: sum_at_owner(): parts = lax.all_to_all(split_up(x, dim, count), axis, 0, 0, tiled=True)]
    pallas_call x0 -> x1, Pallas kernels: none -> 104 us  [shards(): pl.pallas_call(functools.partial(kernel, n, n_tp, hu, fd), out_shape=(jax...]
    all_to_all x9 -> x0, starting transfers between devices: 71.8 us -> none  [the longest x2 30.2 us: relayout(): lax.all_to_all(down_part, 'fs', split_axis=0, concat_axis=1, tiled=True)]
    all_gather x2 -> x0, waiting for transfers between devices: 12.2 us -> none  [sent_together(): out = lax.all_gather(both, axis, axis=dim, tiled=True)]
    dot_general x4 -> x0, matrix products: 10 us -> none  [the longest x2 6.79 us: projector(): return jnp.dot(hidden, down_flat, preferred_element_type=jnp.float32)]
    reshape x9 -> x0, local copies, waits for them, and re-layouts: 8.31 us -> none  [the longest x2 4.49 us: split_up(): return jnp.moveaxis(x.reshape(*before, count, -1, *after), dim, 0)]
    unnamed x40 -> x9, local copies, waits for them, and re-layouts: 12.4 us -> 6.34 us
    split x2 -> x0, local copies, waits for them, and re-layouts: 4.02 us -> none  [sent_together(): jnp.split(out, [sum(widths[:k]) for k in range(1, len(widths))], axis=along)]
  transfers between devices with their start and end apart: 11 -> 0, of which waited for: 9 -> 0; matrix products, arithmetic and copies ran while one was open for 12% -> 0% of each run, Pallas kernels for 0% -> 0%
where the time goes in v1:
time: 114 us; the launch traced here: 113 us
  Pallas kernels  104 us (91%)
  local copies, waits for them, and re-layouts  8.41 us (7%)
    pallas_call x1, Pallas kernels, shards(): pl.pallas_call(functools.partial(kernel, n, n_tp, hu, fd), out_shape=(jax...  104 us
    unnamed x9, local copies, waits for them, and re-layouts  6.34 us

profile of v1, /device:TPU:8, one launch (start us, length us, event | category | flops | bytes accessed | tf_op | source)
XLA Modules:
  0.0 113.5 jit_solution(2934850395876773145)
XLA Ops:
  0.6 104.4 %shard_map.144 = (bf16[4,2048]{1,0:T(4,128)(2,1)}, bf16[2,8,3,16,2048]{4,3,2,1,0:T(8,128)(2,1)}) custom-call(bf16[256,2048]{1,0:T(8,128)(2,1)} %bitcast.16, f32[1,32]{1,0:T(1,128)} %bitcast.18, f32[32,704]{1,0:T(8,128)} %gate_one.1, f32[32,704]{1,0:T(8,128)} %up_one.1, f32[32,704]{1,0:T(8,128)} %down_one.1, f32[1,32]{1,0:T(1,128)} %bitcast.19, ...), custom_call_target="tpu_custom_call" | custom-call | tf_op jit(solution)/shard_map/pallas_call | solution.py:300
  105.1 2.1 %slice_bitcast_fusion = (bf16[8,11,2048]{2,1,0:T(8,128)(2,1)S(1)}, bf16[8,11,2048]{2,1,0:T(8,128)(2,1)S(1)}, bf16[8,11,2048]{2,1,0:T(8,128)(2,1)S(1)}, bf16[8,11...) fusion(bf16[2,8,3,16,2048]{4,3,2,1,0:T(8,128)(2,1)} %get-tuple-element.10), kind=kLoop, calls=%fused_computation | loop fusion | bytes 4325376 | tf_op jit(solution)/shard_map/squeeze | solution.py:335
  107.1 0.0 copy-start
  107.1 1.0 copy.21
  108.1 1.0 copy.20
  109.1 1.0 copy.19
  110.0 1.0 copy.18
  111.0 1.0 copy.17
  111.9 1.0 copy.16
  112.9 0.0 copy-done
  112.9 0.6 copy.23
Async XLA Ops:
  107.1 5.7 %copy-start = (bf16[4,2048]{1,0:T(4,128)(2,1)S(1)}, bf16[4,2048]{1,0:T(4,128)(2,1)}, u32[]{:S(2)}) copy-start(bf16[4,2048]{1,0:T(4,128)(2,1)} %get-tuple-element.9) | copy-start | bytes 49156

commit v2 on v1

--- a/solution.py
+++ b/solution.py
@@ -20,13 +20,14 @@
 
 def kernel(
     n, n_tp, hu, fd,
-    tokens, gain_one, gate_one, up_one, down_one, gain_two, gate_two, up_two, down_two,
-    mixed, served,
-    stack, turned, outgoing, incoming, weights, hidden, normed, part, landed, group, owner,
-    small, gathered, middle,
+    tokens_hbm, gain_one, gate_one, up_one, down_one, gain_two, gate_two, up_two, down_two,
+    mixed, out_0, out_1, out_2, out_3, out_4, out_5,
+    tokens, gains, trained, stack, turned, outgoing, incoming, weights, hidden, normed, part, landed, group, owner,
+    small, gathered, middle, staged,
     w_send, w_recv, x_send, x_recv, r_send, ra_recv, rb_recv, q_send, q_recv,
-    s_send, s_recv, g_send, ga_recv, gb_recv, out_sem,
+    s_send, s_recv, g_send, ga_recv, gb_recv, in_sem, out_sem,
 ):
+    served = (out_0, out_1, out_2, out_3, out_4, out_5)
     fs = n * n
     d = fs * fd
     half = OWN * fs // 2
@@ -49,6 +50,16 @@
     def drain(ref, sem):
         pltpu.make_async_copy(ref, ref, sem).wait()
 
+    given = ((gain_one, gate_one, up_one, down_one), (gain_two, gate_two, up_two, down_two))
+    loads = []
+    for b, (gain, *each) in enumerate(given):
+        loads.append(pltpu.make_async_copy(gain, gains.at[b], in_sem.at[b, 3]))
+        for w in range(3):
+            loads.append(pltpu.make_async_copy(each[w], trained.at[b, w], in_sem.at[b, w]))
+    loads.append(pltpu.make_async_copy(tokens_hbm, tokens, in_sem.at[0, 4]))
+    for load in loads:
+        load.start()
+
     barrier = pltpu.get_barrier_semaphore()
 
     @pl.loop(1, fs)
@@ -63,15 +74,14 @@
     pl.semaphore_signal(barrier, inc=1, device_id=partner, device_id_type=MESH)
 
     hidden_units = gate_one.shape[1]
-    for b, (gain, gate, up, down) in enumerate(
-        ((gain_one, gate_one, up_one, down_one), (gain_two, gate_two, up_two, down_two))
-    ):
-        stack[...] = jnp.zeros_like(stack)
-        stack[0:fd, 0:hidden_units] = gate[...]
-        stack[fd : 2 * fd, 0:hidden_units] = up[...]
-        stack[2 * fd : 3 * fd, 0:hidden_units] = down[...]
+    stack[...] = jnp.zeros_like(stack)
+    for b in range(2):
+        for load in loads[4 * b : 4 * b + 4]:
+            load.wait()
+        for w in range(3):
+            stack[w * fd : (w + 1) * fd, 0:hidden_units] = trained[b, w]
         ones = jnp.ones((1, fd), F32)
-        scale = jnp.concatenate([gain[...], gain[...], ones, ones], axis=1)
+        scale = jnp.concatenate([gains[b], gains[b], ones, ones], axis=1)
         turned[...] = stack[...].T * scale
         live = lax.broadcasted_iota(jnp.int32, (ROWS, 128), 0) < hu
         for k in range(fs):
@@ -97,6 +107,7 @@
             outgoing.at[b, f], incoming.at[b, lax.rem(f, 4), f // 4], w_recv.at[b]
         ).start()
 
+    loads[8].wait()
     wide = tokens[...].astype(F32)
     normed_rows = rsqrt_norm(wide)
     spot = lax.broadcasted_iota(jnp.int32, (2 * half, 2 * half), 0)
@@ -157,8 +168,20 @@
         for k in range(2 * nx - 1):
             drain(weights.at[b, t], x_send.at[b, k])
 
+    def shipped(b, w):
+        return pltpu.make_async_copy(staged.at[3 * b + w], served[3 * b + w], out_sem.at[b, w])
+
     def publish(b):
-        return pltpu.make_async_copy(weights.at[b], served.at[b], out_sem.at[b])
+        width = hu * n_tp
+        spot = lax.broadcasted_iota(jnp.int32, (width, n_tp * ROWS), 0)
+        source = lax.broadcasted_iota(jnp.int32, (width, n_tp * ROWS), 1)
+        swap = jnp.where(source == spot % n_tp * ROWS + spot // n_tp, 1.0, 0.0).astype(BF16)
+        for w in range(3):
+            held = weights[b, :, w].reshape(n_tp * ROWS, d)
+            rows = jnp.dot(swap, held, preferred_element_type=F32)
+            for r in range(hu):
+                staged[3 * b + w, r] = rows[r * n_tp : (r + 1) * n_tp].astype(BF16)
+            shipped(b, w).start()
 
     def feed(b, side):
         rows = normed[side * half : (side + 1) * half, :]
@@ -224,12 +247,12 @@
 
     exchange(0)
     hand_over(0)
-    exchange(1)
     collected(0)
-    publish(0).start()
     for side in range(2):
         feed(0, side)
         send_blocks(0, side)
+    exchange(1)
+    publish(0)
     hand_over(1)
     for side in range(2):
         reduce_blocks(0, side)
@@ -264,13 +287,13 @@
             ).start()
 
     collected(1)
-    publish(1).start()
     for side in range(2):
         recv = ga_recv if side == 0 else gb_recv
         drain(gathered.at[side, pl.ds(0, n - 1)], recv)
         normed[side * half : (side + 1) * half, :] = gathered[side].reshape(half, d)
         feed(1, side)
         send_blocks(1, side)
+    publish(1)
     for side in range(2):
         reduce_blocks(1, side)
     mixed[...] = (mid + 0.5 * summed(1)).astype(BF16)
@@ -281,7 +304,22 @@
         drain(outgoing.at[b, pl.ds(0, fs - 1)], w_send.at[b])
         drain(part.at[b, pl.ds(0, 2 * n - 2)], r_send.at[b])
         drain(owner.at[b, pl.ds(0, n - 1)], q_send.at[b])
-        publish(b).wait()
+        for w in range(3):
+            shipped(b, w).wait()
+
+
+def deliver(count, *refs):
+    sources, targets, held = refs[:count], refs[count : 2 * count], refs[2 * count : 3 * count]
+    in_sem, out_sem = refs[3 * count :]
+    taken = [pltpu.make_async_copy(sources[k], held[k], in_sem.at[k]) for k in range(count)]
+    given = [pltpu.make_async_copy(held[k], targets[k], out_sem.at[k]) for k in range(count)]
+    for copy in taken:
+        copy.start()
+    for k in range(count):
+        taken[k].wait()
+        given[k].start()
+    for copy in given:
+        copy.wait()
 
 
 def shards(
@@ -296,16 +334,20 @@
     block = rows // 2 // n
     wide = -(-(local + ROWS) // 128) * 128
     vmem = pl.BlockSpec(memory_space=pltpu.VMEM)
+    hbm = pl.BlockSpec(memory_space=pltpu.HBM)
     dma, one = pltpu.SemaphoreType.DMA, (2,)
-    mixed, served = pl.pallas_call(
+    results = pl.pallas_call(
         functools.partial(kernel, n, n_tp, hu, fd),
         out_shape=(
             jax.ShapeDtypeStruct((OWN, d), BF16),
-            jax.ShapeDtypeStruct((2, n_tp, 3, ROWS, d), BF16),
-        ),
-        in_specs=[vmem] * 9,
-        out_specs=(vmem, pl.BlockSpec(memory_space=pl.ANY)),
+        )
+        + (jax.ShapeDtypeStruct((hu, n_tp, d), BF16),) * 6,
+        in_specs=[hbm] * 9,
+        out_specs=(vmem,) + (hbm,) * 6,
         scratch_shapes=[
+            pltpu.VMEM((rows, d), BF16),
+            pltpu.VMEM((2, 1, fd), F32),
+            pltpu.VMEM((2, 3, fd, local), F32),
             pltpu.VMEM((4 * fd, wide), F32),
             pltpu.VMEM((wide, 4 * fd), F32),
             pltpu.VMEM((2, fs, ROWS, 128), BF16),
@@ -320,19 +362,27 @@
             pltpu.VMEM((n, OWN, d), BF16),
             pltpu.VMEM((2, n, block, d), BF16),
             pltpu.VMEM((OWN, d), BF16),
+            pltpu.VMEM((6, hu, n_tp, d), BF16),
             dma(one), dma(one), dma((2, n_tp - 1)), dma((2, n_tp)),
             dma(one), dma(one), dma(one), dma(one), dma(one),
-            dma(()), dma(()), dma(()), dma(()), dma(()), dma(one),
+            dma(()), dma(()), dma(()), dma(()), dma(()), dma((2, 5)), dma((2, 3)),
         ],
         compiler_params=pltpu.CompilerParams(
-            collective_id=0, has_side_effects=True, vmem_limit_bytes=60 * 1024 * 1024
+            collective_id=0, has_side_effects=True, vmem_limit_bytes=67043328
         ),
     )(
         tokens[0],
         gain_first[None], gate_first, up_first, down_first,
         gain_second[None], gate_second, up_second, down_second,
     )
-    return (mixed[None],) + tuple(served[b, :, w, :hu, :] for b in range(2) for w in range(3))
+    mixed, *served = pl.pallas_call(
+        functools.partial(deliver, 7),
+        out_shape=tuple(jax.ShapeDtypeStruct(r.shape, r.dtype) for r in results),
+        in_specs=[hbm] * 7,
+        out_specs=(hbm,) * 7,
+        scratch_shapes=[pltpu.VMEM(r.shape, r.dtype) for r in results] + [dma((7,)), dma((7,))],
+    )(*results)
+    return (mixed[None],) + tuple(jnp.swapaxes(r, 0, 1) for r in served)
 
 
 def solution(mesh):

time: 114 us -> 105 us (0.921)
  the two profiles are of different devices: /device:TPU:8 before, /device:TPU:80 now
where the time goes in v2:
time: 105 us
  Pallas kernels  104 us (99%)
    pallas_call x1, Pallas kernels, shards(): pl.pallas_call(functools.partial(kernel, n, n_tp, hu, fd), out_shape=(jax...  102 us
    pallas_call x1, Pallas kernels, shards(): pl.pallas_call(functools.partial(deliver, 7), out_shape=tuple((jax.ShapeD...  2.45 us

profile of v2, /device:TPU:80, one launch (start us, length us, event | category | flops | bytes accessed | tf_op | source)
XLA Modules:
  0.0 104.7 jit_solution(453488779329617423)
XLA Ops:
  0.6 101.6 %shard_map.144 = (bf16[4,2048]{1,0:T(4,128)(2,1)}, bf16[11,8,2048]{2,1,0:T(8,128)(2,1)}, bf16[11,8,2048]{2,1,0:T(8,128)(2,1)}, bf16[11,8,2048]{2,1,0:T(8,128)(2,...) custom-call(bf16[256,2048]{1,0:T(8,128)(2,1)} %bitcast.10, ...), custom_call_target="tpu_custom_call" | custom-call | tf_op jit(solution)/shard_map/pallas_call | solution.py:339
  102.3 2.5 %shard_map.145 = (bf16[4,2048]{1,0:T(4,128)(2,1)}, bf16[11,8,2048]{2,1,0:T(8,128)(2,1)}, bf16[11,8,2048]{2,1,0:T(8,128)(2,1)}, bf16[11,8,2048]{2,1,0:T(8,128)(2,...) custom-call(bf16[4,2048]{1,0:T(4,128)(2,1)} %get-tuple-element.21.refs_0_, ...), custom_call_target="tpu_custom_call" | custom-call | tf_op jit(solution)/shard_map/pallas_call | solution.py:378

commit v3 on v2

v3 whole, which is shorter than its diff:
```python
import functools

import jax
import jax.numpy as jnp
from jax import lax
from jax.experimental import pallas as pl
from jax.experimental.pallas import tpu as pltpu
from jax.sharding import PartitionSpec as P

MESH = pl.DeviceIdType.MESH
F32, BF16 = jnp.float32, jnp.bfloat16
ROWS = 16
OWN = 4


def rsqrt_norm(wide):
    scale = lax.rsqrt(jnp.mean(wide * wide, axis=-1, keepdims=True) + 1e-06)
    return (wide * scale).astype(BF16)


def kernel(
    n, n_tp, hu, fd,
    tokens_hbm, gain_one, gate_one, up_one, down_one, gain_two, gate_two, up_two, down_two,
    mixed, out_0, out_1, out_2, out_3, out_4, out_5,
    tokens, gains, trained, stack, turned, outgoing, incoming, weights, normed,
    part, landed, group, owner, small, gathered_a, gathered_b, part_a, part_b, landed_a, landed_b,
    group_a, group_b, owner_two, middle, staged,
    w_send, w_recv, x_send, x_recv, half_recv, pair_send, pair_recv, r_send, ra_recv, rb_recv,
    q_send, q_recv, s_send, s_recv, g_send, ga_recv, gb_recv, in_sem, out_sem,
):
    served = (out_0, out_1, out_2, out_3, out_4, out_5)
    fs = n * n
    d = fs * fd
    half = OWN * fs // 2
    block = half // n
    groups = n // 2
    m = n // 2
    f, t = lax.axis_index("fs"), lax.axis_index("tp")
    z, y = f // n, lax.rem(f, n)
    e, q = lax.rem(y, 2), y // 2
    x, c = t // 2, lax.rem(t, 2)
    nx = n_tp // 2
    even = lax.rem(z + y, 2) == 0
    even_two = lax.rem(z + q, 2) == 0
    partner = (f, x * 2 + 1 - c)

    def at(zz, yy):
        return (zz * n + yy, t)

    def at_two(zz, qq):
        return (zz * n + 2 * qq + e, t)

    def along(step):
        return (f, lax.rem(x + nx + step, nx) * 2 + c)

    def slot_of(step, core):
        return lax.rem(x + nx + step, nx) * 2 + core

    def remote(src, dst, send, recv, device):
        return pltpu.make_async_remote_copy(
            src_ref=src, dst_ref=dst, send_sem=send, recv_sem=recv, device_id=device, device_id_type=MESH
        )

    def drain(ref, sem):
        pltpu.make_async_copy(ref, ref, sem).wait()

    given = ((gain_one, gate_one, up_one, down_one), (gain_two, gate_two, up_two, down_two))
    loads = []
    for b, (gain, *each) in enumerate(given):
        loads.append(pltpu.make_async_copy(gain, gains.at[b], in_sem.at[b, 3]))
        for w in range(3):
            loads.append(pltpu.make_async_copy(each[w], trained.at[b, w], in_sem.at[b, w]))
    loads.append(pltpu.make_async_copy(tokens_hbm, tokens, in_sem.at[0, 4]))
    for load in loads:
        load.start()
    owner_two[...] = jnp.zeros_like(owner_two)

    barrier = pltpu.get_barrier_semaphore()

    @pl.loop(1, fs)
    def _(k):
        pl.semaphore_signal(barrier, inc=1, device_id=(lax.rem(f + k, fs), t), device_id_type=MESH)

    around = {1: (), 2: (1,), 4: (1, -1)}[nx]
    for step in around:
        pl.semaphore_signal(barrier, inc=1, device_id=along(step), device_id_type=MESH)
    pl.semaphore_signal(barrier, inc=1, device_id=partner, device_id_type=MESH)

    hidden_units = gate_one.shape[1]
    stack[...] = jnp.zeros_like(stack)
    for b in range(2):
        for load in loads[4 * b : 4 * b + 4]:
            load.wait()
        for w in range(3):
            stack[w * fd : (w + 1) * fd, 0:hidden_units] = trained[b, w]
        ones = jnp.ones((1, fd), F32)
        scale = jnp.concatenate([gains[b], gains[b], ones, ones], axis=1)
        turned[...] = stack[...].T * scale
        live = lax.broadcasted_iota(jnp.int32, (ROWS, 128), 0) < hu
        for k in range(fs):
            rows = turned[k * hu : k * hu + ROWS, :]
            outgoing[b, k] = jnp.where(live, rows, 0.0).astype(BF16)

    pl.semaphore_wait(barrier, fs - 1 + len(around) + 1)

    for b in range(2):

        @pl.loop(1, fs)
        def _(k):
            peer = lax.rem(f + k, fs)
            remote(
                outgoing.at[b, peer],
                incoming.at[b, lax.rem(f, 4), f // 4],
                w_send.at[b],
                w_recv.at[b],
                (peer, t),
            ).start()

        pltpu.make_async_copy(
            outgoing.at[b, f], incoming.at[b, lax.rem(f, 4), f // 4], w_recv.at[b]
        ).start()

    loads[8].wait()
    wide = tokens[...].astype(F32)
    normed_rows = rsqrt_norm(wide)
    spot = lax.broadcasted_iota(jnp.int32, (2 * half, 2 * half), 0)
    source = lax.broadcasted_iota(jnp.int32, (2 * half, 2 * half), 1)
    in_first = spot < half
    inside = jnp.where(in_first, spot, spot - half)
    major = inside // block
    minor = (inside % block) // OWN
    row = inside % OWN
    first_home = major * n + 2 * minor + major % 2
    second_home = (2 * minor + (major + 1) % 2) * n + major
    home = jnp.where(in_first, first_home, second_home) * OWN + row
    shuffle = jnp.where(home == source, 1.0, 0.0).astype(BF16)
    normed[...] = jnp.dot(shuffle, normed_rows, preferred_element_type=F32).astype(BF16)
    pick_row = lax.broadcasted_iota(jnp.int32, (8, 2 * half), 0)
    pick_source = lax.broadcasted_iota(jnp.int32, (8, 2 * half), 1)
    pick = jnp.where((pick_row < OWN) & (pick_source == pick_row + f * OWN), 1.0, 0.0).astype(BF16)
    mine = jnp.dot(pick, tokens[...], preferred_element_type=F32)[0:OWN]

    lanes = 3 * 128
    lane_in = lax.broadcasted_iota(jnp.int32, (128, lanes), 0)
    lane_out = lax.broadcasted_iota(jnp.int32, (128, lanes), 1)
    inner = lane_out % 128

    def merge(b):
        drain(incoming.at[b], w_recv.at[b])
        total = jnp.zeros((fs // 4 * ROWS, lanes), F32)
        for i in range(4):
            chosen = (inner // 32 == i) & (lane_in == lane_out // 128 * 32 + inner % 32)
            spread_out = jnp.where(chosen, 1.0, 0.0).astype(BF16)
            piece = incoming[b, i].reshape(fs // 4 * ROWS, 128)
            total = total + jnp.dot(piece, spread_out, preferred_element_type=F32)
        merged = total.astype(BF16)
        for j in range(fs // 4):
            for w in range(3):
                weights[b, t, w, :, j * 128 : (j + 1) * 128] = merged[
                    j * ROWS : (j + 1) * ROWS, w * 128 : (w + 1) * 128
                ]

    def part_of(s, slot, h):
        return weights.at[s, slot, :, :, h * (d // 2) : (h + 1) * (d // 2)]

    def spread(s):
        for step in around:
            remote(weights.at[s, t], weights.at[s, t], x_send.at[s], x_recv.at[s, t], along(step)).start()
        remote(weights.at[s, t], weights.at[s, t], x_send.at[s], x_recv.at[s, t], partner).start()

    def relay(s):
        for h, step in enumerate(around):
            slot = slot_of(-step, c)
            drain(weights.at[s, slot], x_recv.at[s, slot])
            if nx == 4:
                remote(
                    part_of(s, slot, h), part_of(s, slot, h), x_send.at[s], half_recv.at[s, h], along(step)
                ).start()
            remote(
                weights.at[s, slot], weights.at[s, slot], x_send.at[s], x_recv.at[s, slot], partner
            ).start()

    def finish(s):
        if nx == 4:
            slot = slot_of(2, c)
            for h in range(2):
                drain(part_of(s, slot, h), half_recv.at[s, h])
                remote(
                    part_of(s, slot, h), part_of(s, slot, h), x_send.at[s], x_recv.at[s, slot], partner
                ).start()

    def collected(s):
        for k in range(nx):
            slot = slot_of(k, 1 - c)
            drain(weights.at[s, slot], x_recv.at[s, slot])

    def shipped(b, w):
        return pltpu.make_async_copy(staged.at[3 * b + w], served[3 * b + w], out_sem.at[b, w])

    def publish(b):
        width = hu * n_tp
        spot = lax.broadcasted_iota(jnp.int32, (width, n_tp * ROWS), 0)
        source = lax.broadcasted_iota(jnp.int32, (width, n_tp * ROWS), 1)
        swap = jnp.where(source == spot % n_tp * ROWS + spot // n_tp, 1.0, 0.0).astype(BF16)
        for w in range(3):
            held = weights[b, :, w].reshape(n_tp * ROWS, d)
            rows = jnp.dot(swap, held, preferred_element_type=F32)
            for r in range(hu):
                staged[3 * b + w, r] = rows[r * n_tp : (r + 1) * n_tp].astype(BF16)
            shipped(b, w).start()

    contract = (((1,), (1,)), ((), ()))

    def branch_of(rows, sets):
        gate, up, down = [
            jnp.concatenate([weights[s, :, w].reshape(n_tp * ROWS, d) for s in sets], axis=0)
            for w in range(3)
        ]
        gate_act = lax.dot_general(rows, gate, contract, preferred_element_type=F32)
        up_act = lax.dot_general(rows, up, contract, preferred_element_type=F32)
        act = (gate_act / (1.0 + jnp.exp(-gate_act)) * up_act).astype(BF16)
        return jnp.dot(act, down, preferred_element_type=F32).astype(BF16)

    def send_blocks(source, target, me, count, send, recv, device):
        @pl.loop(1, count)
        def _(k):
            peer = lax.rem(me + k, count)
            remote(source.at[peer], target.at[me], send, recv, device(peer)).start()

        pltpu.make_async_copy(source.at[me], target.at[me], recv).start()

    def reduced(target, count, recv):
        drain(target, recv)
        total = target[0].astype(F32)
        for k in range(1, count):
            total = total + target[k].astype(F32)
        return total

    def hand_groups(total, held, targets, me, own, send, recv, device):
        for k, peer in enumerate(targets):
            held[k] = total[k * OWN : (k + 1) * OWN].astype(BF16)

            @pl.when(peer != me)
            def _():
                remote(held.at[k], own.at[me], send, recv, device(peer)).start()

            @pl.when(peer == me)
            def _():
                pltpu.make_async_copy(held.at[k], own.at[me], recv).start()

    def added(own):
        total = own[0].astype(F32)
        for k in range(1, n):
            total = total + own[k].astype(F32)
        return total

    merge(0)
    spread(0)
    relay(0)
    finish(0)
    collected(0)
    for side in range(2):
        rows = normed[side * half : (side + 1) * half, :]
        part[side * n : (side + 1) * n] = branch_of(rows, (0,)).reshape(n, block, d)
        send_blocks(
            part.at[pl.ds(side * n, n)],
            landed.at[side],
            z if side == 0 else y,
            n,
            r_send.at[0],
            (ra_recv if side == 0 else rb_recv).at[0],
            (lambda peer: at(peer, y)) if side == 0 else (lambda peer: at(z, peer)),
        )
    merge(1)
    spread(1)
    twin = (z * n + y + 1 - 2 * e, t)
    remote(weights.at[1, t], weights.at[2, t], pair_send, pair_recv, twin).start()
    publish(0)
    drain(weights.at[2, t], pair_recv)
    spread(2)
    total = reduced(landed.at[0], n, ra_recv.at[0])
    hand_groups(
        total, group.at[0], [2 * k + lax.rem(z, 2) for k in range(groups)], y,
        owner, q_send.at[0], q_recv.at[0], lambda peer: at(z, peer),
    )
    total = reduced(landed.at[1], n, rb_recv.at[0])
    hand_groups(
        total, group.at[1], [2 * k + lax.rem(y + 1, 2) for k in range(groups)], z,
        owner, q_send.at[0], q_recv.at[0], lambda peer: at(peer, y),
    )
    relay(1)
    drain(owner, q_recv.at[0])
    middle[...] = (mine + 0.5 * added(owner)).astype(BF16)
    mid = middle[...].astype(F32)
    own_slot = jnp.where(even_two, q // 2, m // 2 + z // 2)
    small[own_slot] = rsqrt_norm(mid)
    for k in range(1, n):
        peer = jnp.where(even_two, z * n + 2 * lax.rem(q + k, m) + e, lax.rem(z + k, n) * n + y)

        def tell():
            remote(small.at[own_slot], small.at[own_slot], s_send, s_recv, (peer, t)).start()

        if k < m:
            tell()
        else:
            pl.when(jnp.logical_not(even_two))(tell)
    finish(1)
    drain(small.at[pl.ds(0, m // 2 + groups - 1)], s_recv)
    rows = jnp.concatenate([small[k].astype(F32) for k in range(m // 2)], axis=0)
    gathered_a[z] = rows.astype(BF16)
    rows = jnp.concatenate([small[m // 2 + k].astype(F32) for k in range(groups)], axis=0)
    gathered_b[q] = rows.astype(BF16)

    @pl.loop(1, n)
    def _(k):
        remote(
            gathered_a.at[z], gathered_a.at[z], g_send.at[0], ga_recv, at_two(lax.rem(z + k, n), q)
        ).start()

    @pl.loop(1, m)
    def _(k):
        remote(
            gathered_b.at[q], gathered_b.at[q], g_send.at[1], gb_recv, at_two(z, lax.rem(q + k, m))
        ).start()

    relay(2)
    finish(2)
    collected(1)
    collected(2)
    drain(gathered_a.at[pl.ds(0, n - 1)], ga_recv)
    drain(gathered_b.at[pl.ds(0, m - 1)], gb_recv)
    quarter = half // 2
    rows = jnp.concatenate(
        [gathered_a[...].reshape(quarter, d), gathered_b[...].reshape(quarter, d)], axis=0
    )
    branch = branch_of(rows, (1, 2))
    part_a[...] = branch[0:quarter].reshape(part_a.shape)
    part_b[...] = branch[quarter:].reshape(part_b.shape)
    send_blocks(part_a, landed_a, z, n, r_send.at[1], ra_recv.at[1], lambda peer: at_two(peer, q))
    send_blocks(part_b, landed_b, q, m, r_send.at[2], rb_recv.at[1], lambda peer: at_two(z, peer))
    publish(1)
    total = reduced(landed_a, n, ra_recv.at[1])
    hand_groups(
        total, group_a, [2 * k + lax.rem(z, 2) for k in range(m // 2)], q,
        owner_two, q_send.at[1], q_recv.at[1], lambda peer: at_two(z, peer),
    )
    total = reduced(landed_b, m, rb_recv.at[1])
    hand_groups(
        total, group_b, [2 * k + lax.rem(q + 1, 2) for k in range(groups)], z,
        owner_two, q_send.at[1], q_recv.at[1], lambda peer: at_two(peer, q),
    )

    @pl.when(even_two)
    def _():
        drain(owner_two.at[pl.ds(0, m)], q_recv.at[1])
        drain(small.at[pl.ds(0, m - 1)], s_send)

    @pl.when(jnp.logical_not(even_two))
    def _():
        drain(owner_two, q_recv.at[1])
        drain(owner.at[pl.ds(0, n - 1)], s_send)

    mixed[...] = (mid + 0.5 * added(owner_two)).astype(BF16)

    drain(weights.at[2, t], pair_send)
    for s in range(3):
        drain(weights.at[s, pl.ds(0, n_tp - 1)], x_send.at[s])
    drain(gathered_a.at[pl.ds(0, n - 1)], g_send.at[0])
    drain(gathered_b.at[pl.ds(0, m - 1)], g_send.at[1])
    drain(part.at[pl.ds(0, 2 * n - 2)], r_send.at[0])
    drain(part_a.at[pl.ds(0, n - 1)], r_send.at[1])
    drain(part_b.at[pl.ds(0, m - 1)], r_send.at[2])
    drain(owner.at[pl.ds(0, n - 1)], q_send.at[0])
    drain(owner_two.at[pl.ds(0, m // 2 + groups - 1)], q_send.at[1])
    for b in range(2):
        drain(outgoing.at[b, pl.ds(0, fs - 1)], w_send.at[b])
        for w in range(3):
            shipped(b, w).wait()


def deliver(count, *refs):
    sources, targets, held = refs[:count], refs[count : 2 * count], refs[2 * count : 3 * count]
    in_sem, out_sem = refs[3 * count :]
    taken = [pltpu.make_async_copy(sources[k], held[k], in_sem.at[k]) for k in range(count)]
    given = [pltpu.make_async_copy(held[k], targets[k], out_sem.at[k]) for k in range(count)]
    for copy in taken:
        copy.start()
    for k in range(count):
        taken[k].wait()
        given[k].start()
    for copy in given:
        copy.wait()


def shards(
    tokens, gain_first, gate_first, up_first, down_first, gain_second, gate_second, up_second, down_second
):
    fs, n_tp = lax.axis_size("fs"), lax.axis_size("tp")
    n = int(round(fs**0.5))
    fd, local = gate_first.shape
    hu = local // fs
    d = fs * fd
    rows = tokens.shape[1]
    block = rows // 2 // n
    wide = -(-(local + ROWS) // 128) * 128
    vmem = pl.BlockSpec(memory_space=pltpu.VMEM)
    hbm = pl.BlockSpec(memory_space=pltpu.HBM)
    dma = pltpu.SemaphoreType.DMA
    m = n // 2
    shape_a = (n, OWN * m // 2, d)
    shape_b = (m, OWN * n // 2, d)
    results = pl.pallas_call(
        functools.partial(kernel, n, n_tp, hu, fd),
        out_shape=(
            jax.ShapeDtypeStruct((OWN, d), BF16),
        )
        + (jax.ShapeDtypeStruct((hu, n_tp, d), BF16),) * 6,
        in_specs=[hbm] * 9,
        out_specs=(vmem,) + (hbm,) * 6,
        scratch_shapes=[
            pltpu.VMEM((rows, d), BF16),
            pltpu.VMEM((2, 1, fd), F32),
            pltpu.VMEM((2, 3, fd, local), F32),
            pltpu.VMEM((4 * fd, wide), F32),
            pltpu.VMEM((wide, 4 * fd), F32),
            pltpu.VMEM((2, fs, ROWS, 128), BF16),
            pltpu.VMEM((2, 4, fs // 4, ROWS, 128), BF16),
            pltpu.VMEM((3, n_tp, 3, ROWS, d), BF16),
            pltpu.VMEM((rows, d), BF16),
            pltpu.VMEM((2 * n, block, d), BF16),
            pltpu.VMEM((2, n, block, d), BF16),
            pltpu.VMEM((2, m, OWN, d), BF16),
            pltpu.VMEM((n, OWN, d), BF16),
            pltpu.VMEM((m // 2 + m, OWN, d), BF16),
            pltpu.VMEM(shape_a, BF16),
            pltpu.VMEM(shape_b, BF16),
            pltpu.VMEM(shape_a, BF16),
            pltpu.VMEM(shape_b, BF16),
            pltpu.VMEM(shape_a, BF16),
            pltpu.VMEM(shape_b, BF16),
            pltpu.VMEM((m // 2, OWN, d), BF16),
            pltpu.VMEM((m, OWN, d), BF16),
            pltpu.VMEM((n, OWN, d), BF16),
            pltpu.VMEM((OWN, d), BF16),
            pltpu.VMEM((6, hu, n_tp, d), BF16),
            dma((2,)), dma((2,)), dma((3,)), dma((3, n_tp)), dma((3, 2)), dma(()), dma(()),
            dma((3,)), dma((2,)), dma((2,)), dma((2,)), dma((2,)), dma(()), dma(()),
            dma((2,)), dma(()), dma(()), dma((2, 5)), dma((2, 3)),
        ],
        compiler_params=pltpu.CompilerParams(
            collective_id=0, has_side_effects=True, vmem_limit_bytes=67043328
        ),
    )(
        tokens[0],
        gain_first[None], gate_first, up_first, down_first,
        gain_second[None], gate_second, up_second, down_second,
    )
    mixed, *served = pl.pallas_call(
        functools.partial(deliver, 7),
        out_shape=tuple(jax.ShapeDtypeStruct(r.shape, r.dtype) for r in results),
        in_specs=[hbm] * 7,
        out_specs=(hbm,) * 7,
        scratch_shapes=[pltpu.VMEM(r.shape, r.dtype) for r in results] + [dma((7,)), dma((7,))],
    )(*results)
    return (mixed[None],) + tuple(jnp.swapaxes(r, 0, 1) for r in served)


def solution(mesh):
    weight = P("fs", "tp")
    cut = P(None, "fs", None)
    return jax.shard_map(
        shards,
        mesh=mesh,
        in_specs=(P("tp", None, None), P("fs"), weight, weight, weight, P("fs"), weight, weight, weight),
        out_specs=(P("tp", "fs", None),) + (cut,) * 6,
        check_vma=False,
    )
```

time: 105 us -> 94.6 us (0.901)
  the two profiles are of different devices: /device:TPU:80 before, /device:TPU:70 now
where the time goes in v3:
time: 94.6 us; the launch traced here: 94.4 us
  Pallas kernels  93.7 us (99%)
    pallas_call x1, Pallas kernels, shards(): pl.pallas_call(functools.partial(kernel, n, n_tp, hu, fd), out_shape=(jax...  91.3 us
    pallas_call x1, Pallas kernels, shards(): pl.pallas_call(functools.partial(deliver, 7), out_shape=tuple((jax.ShapeD...  2.45 us

profile of v3, /device:TPU:70, one launch (start us, length us, event | category | flops | bytes accessed | tf_op | source)
XLA Modules:
  0.0 94.4 jit_solution(5521548528826577424)
XLA Ops:
  0.6 91.3 %shard_map.144 = (bf16[4,2048]{1,0:T(4,128)(2,1)}, bf16[11,8,2048]{2,1,0:T(8,128)(2,1)}, bf16[11,8,2048]{2,1,0:T(8,128)(2,1)}, bf16[11,8,2048]{2,1,0:T(8,128)(2,...) custom-call(bf16[256,2048]{1,0:T(8,128)(2,1)} %bitcast.10, ...), custom_call_target="tpu_custom_call" | custom-call | tf_op jit(solution)/shard_map/pallas_call | solution.py:412
  91.9 2.5 %shard_map.145 = (bf16[4,2048]{1,0:T(4,128)(2,1)}, bf16[11,8,2048]{2,1,0:T(8,128)(2,1)}, bf16[11,8,2048]{2,1,0:T(8,128)(2,1)}, bf16[11,8,2048]{2,1,0:T(8,128)(2,...) custom-call(bf16[4,2048]{1,0:T(4,128)(2,1)} %get-tuple-element.21.refs_0_, ...), custom_call_target="tpu_custom_call" | custom-call | tf_op jit(solution)/shard_map/pallas_call | solution.py:458

commit v4 on v3

--- a/solution.py
+++ b/solution.py
@@ -11,6 +11,10 @@
 F32, BF16 = jnp.float32, jnp.bfloat16
 ROWS = 16
 OWN = 4
+
+
+def far_first(count):
+    return sorted(range(1, count), key=lambda k: (-min(k, count - k), k))
 
 
 def rsqrt_norm(wide):
@@ -103,11 +107,11 @@
 
     pl.semaphore_wait(barrier, fs - 1 + len(around) + 1)
 
+    offsets = [(dz, dy) for dz in range(n) for dy in range(n) if dz or dy]
+    offsets.sort(key=lambda o: -(min(o[0], n - o[0]) + min(o[1], n - o[1])))
     for b in range(2):
-
-        @pl.loop(1, fs)
-        def _(k):
-            peer = lax.rem(f + k, fs)
+        for dz, dy in offsets:
+            peer = lax.rem(z + dz, n) * n + lax.rem(y + dy, n)
             remote(
                 outgoing.at[b, peer],
                 incoming.at[b, lax.rem(f, 4), f // 4],
@@ -222,8 +226,7 @@
         return jnp.dot(act, down, preferred_element_type=F32).astype(BF16)
 
     def send_blocks(source, target, me, count, send, recv, device):
-        @pl.loop(1, count)
-        def _(k):
+        for k in far_first(count):
             peer = lax.rem(me + k, count)
             remote(source.at[peer], target.at[me], send, recv, device(peer)).start()
 
@@ -257,6 +260,9 @@
     merge(0)
     spread(0)
     relay(0)
+    merge(1)
+    twin = (z * n + y + 1 - 2 * e, t)
+    remote(weights.at[1, t], weights.at[2, t], pair_send, pair_recv, twin).start()
     finish(0)
     collected(0)
     for side in range(2):
@@ -271,13 +277,11 @@
             (ra_recv if side == 0 else rb_recv).at[0],
             (lambda peer: at(peer, y)) if side == 0 else (lambda peer: at(z, peer)),
         )
-    merge(1)
     spread(1)
-    twin = (z * n + y + 1 - 2 * e, t)
-    remote(weights.at[1, t], weights.at[2, t], pair_send, pair_recv, twin).start()
-    publish(0)
     drain(weights.at[2, t], pair_recv)
     spread(2)
+    publish(0)
+    relay(1)
     total = reduced(landed.at[0], n, ra_recv.at[0])
     hand_groups(
         total, group.at[0], [2 * k + lax.rem(z, 2) for k in range(groups)], y,
@@ -288,7 +292,7 @@
         total, group.at[1], [2 * k + lax.rem(y + 1, 2) for k in range(groups)], z,
         owner, q_send.at[0], q_recv.at[0], lambda peer: at(peer, y),
     )
-    relay(1)
+    relay(2)
     drain(owner, q_recv.at[0])
     middle[...] = (mine + 0.5 * added(owner)).astype(BF16)
     mid = middle[...].astype(F32)
@@ -304,26 +308,21 @@
             tell()
         else:
             pl.when(jnp.logical_not(even_two))(tell)
-    finish(1)
     drain(small.at[pl.ds(0, m // 2 + groups - 1)], s_recv)
     rows = jnp.concatenate([small[k].astype(F32) for k in range(m // 2)], axis=0)
     gathered_a[z] = rows.astype(BF16)
     rows = jnp.concatenate([small[m // 2 + k].astype(F32) for k in range(groups)], axis=0)
     gathered_b[q] = rows.astype(BF16)
 
-    @pl.loop(1, n)
-    def _(k):
+    for k in far_first(n):
         remote(
             gathered_a.at[z], gathered_a.at[z], g_send.at[0], ga_recv, at_two(lax.rem(z + k, n), q)
         ).start()
-
-    @pl.loop(1, m)
-    def _(k):
+    for k in far_first(m):
         remote(
             gathered_b.at[q], gathered_b.at[q], g_send.at[1], gb_recv, at_two(z, lax.rem(q + k, m))
         ).start()
-
-    relay(2)
+    finish(1)
     finish(2)
     collected(1)
     collected(2)

time: 94.6 us -> 88.3 us (0.933)
  the two profiles are of different devices: /device:TPU:70 before, /device:TPU:1 now
where the time goes in v4:
time: 88.3 us; the launch traced here: 88.1 us
  Pallas kernels  87.4 us (99%)
    pallas_call x1, Pallas kernels, shards(): pl.pallas_call(functools.partial(kernel, n, n_tp, hu, fd), out_shape=(jax...  85 us
    pallas_call x1, Pallas kernels, shards(): pl.pallas_call(functools.partial(deliver, 7), out_shape=tuple((jax.ShapeD...  2.45 us

profile of v4, /device:TPU:1, one launch (start us, length us, event | category | flops | bytes accessed | tf_op | source)
XLA Modules:
  0.0 88.1 jit_solution(1793288662803383902)
XLA Ops:
  0.6 85.0 %shard_map.144 = (bf16[4,2048]{1,0:T(4,128)(2,1)}, bf16[11,8,2048]{2,1,0:T(8,128)(2,1)}, bf16[11,8,2048]{2,1,0:T(8,128)(2,1)}, bf16[11,8,2048]{2,1,0:T(8,128)(2,...) custom-call(bf16[256,2048]{1,0:T(8,128)(2,1)} %bitcast.10, ...), custom_call_target="tpu_custom_call" | custom-call | tf_op jit(solution)/shard_map/pallas_call | solution.py:411
  85.6 2.5 %shard_map.145 = (bf16[4,2048]{1,0:T(4,128)(2,1)}, bf16[11,8,2048]{2,1,0:T(8,128)(2,1)}, bf16[11,8,2048]{2,1,0:T(8,128)(2,1)}, bf16[11,8,2048]{2,1,0:T(8,128)(2,...) custom-call(bf16[4,2048]{1,0:T(4,128)(2,1)} %get-tuple-element.21.refs_0_, ...), custom_call_target="tpu_custom_call" | custom-call | tf_op jit(solution)/shard_map/pallas_call | solution.py:457

commit v5 on v4

v5 whole, which is shorter than its diff:
```python
import functools

import jax
import jax.numpy as jnp
from jax import lax
from jax.experimental import pallas as pl
from jax.experimental.pallas import tpu as pltpu
from jax.sharding import PartitionSpec as P

MESH = pl.DeviceIdType.MESH
F32, BF16 = jnp.float32, jnp.bfloat16
ROWS = 16
OWN = 4


def far_first(count):
    return sorted(range(1, count), key=lambda k: (-min(k, count - k), k))


def rsqrt_norm(wide):
    scale = lax.rsqrt(jnp.mean(wide * wide, axis=-1, keepdims=True) + 1e-06)
    return (wide * scale).astype(BF16)


def kernel(
    n, n_tp, hu, fd,
    tokens_hbm, gain_one, gate_one, up_one, down_one, gain_two, gate_two, up_two, down_two,
    mixed, out_0, out_1, out_2, out_3, out_4, out_5,
    tokens, gains, trained, stack, turned, outgoing, incoming, weights_8, weights_4, ready, normed,
    part, landed, group, owner, small, gathered, part_two, landed_two, group_two, owner_two, middle,
    staged,
    w_send, w_recv, x_send, near_recv, half_recv, die_recv, quad_send, quad_recv, r_send, r_recv,
    q_send, q_recv, s_send, s_recv, g_send, g_recv, in_sem, out_sem,
):
    served = (out_0, out_1, out_2, out_3, out_4, out_5)
    fs = n * n
    d = fs * fd
    half = OWN * fs // 2
    block = half // n
    groups = n // 2
    m = n // 2
    f, t = lax.axis_index("fs"), lax.axis_index("tp")
    z, y = f // n, lax.rem(f, n)
    ez, ey, p, q = lax.rem(z, 2), lax.rem(y, 2), z // 2, y // 2
    x, c = t // 2, lax.rem(t, 2)
    nx = n_tp // 2
    even = lax.rem(p + q, 2) == 0
    partner = (f, x * 2 + 1 - c)

    def at(zz, yy):
        return (zz * n + yy, t)

    def at_two(pp, qq):
        return ((2 * pp + ez) * n + 2 * qq + ey, t)

    def along(step):
        return (f, lax.rem(x + nx + step, nx) * 2 + c)

    def slot_of(step, core):
        return lax.rem(x + nx + step, nx) * 2 + core

    def remote(src, dst, send, recv, device):
        return pltpu.make_async_remote_copy(
            src_ref=src, dst_ref=dst, send_sem=send, recv_sem=recv, device_id=device, device_id_type=MESH
        )

    def drain(ref, sem):
        pltpu.make_async_copy(ref, ref, sem).wait()

    given = ((gain_one, gate_one, up_one, down_one), (gain_two, gate_two, up_two, down_two))
    for b, (gain, *each) in enumerate(given):
        pltpu.make_async_copy(gain, gains.at[b], in_sem.at[3]).start()
        for w in range(3):
            pltpu.make_async_copy(each[w], trained.at[b, w], in_sem.at[b]).start()
    pltpu.make_async_copy(tokens_hbm, tokens, in_sem.at[2]).start()

    barrier = pltpu.get_barrier_semaphore()

    @pl.loop(1, fs)
    def _(k):
        pl.semaphore_signal(barrier, inc=1, device_id=(lax.rem(f + k, fs), t), device_id_type=MESH)

    around = {1: (), 2: (1,), 4: (1, -1)}[nx]
    for step in around:
        pl.semaphore_signal(barrier, inc=1, device_id=along(step), device_id_type=MESH)
    pl.semaphore_signal(barrier, inc=1, device_id=partner, device_id_type=MESH)

    hidden_units = gate_one.shape[1]
    stack[...] = jnp.zeros_like(stack)
    drain(gains, in_sem.at[3])
    for b in range(2):
        drain(trained.at[b], in_sem.at[b])
        for w in range(3):
            stack[w * fd : (w + 1) * fd, 0:hidden_units] = trained[b, w]
        ones = jnp.ones((1, fd), F32)
        scale = jnp.concatenate([gains[b], gains[b], ones, ones], axis=1)
        turned[...] = stack[...].T * scale
        live = lax.broadcasted_iota(jnp.int32, (ROWS, 128), 0) < hu
        for k in range(fs):
            rows = turned[k * hu : k * hu + ROWS, :]
            outgoing[b, k] = jnp.where(live, rows, 0.0).astype(BF16)

    pl.semaphore_wait(barrier, fs - 1 + len(around) + 1)

    offsets = [(dz, dy) for dz in range(n) for dy in range(n) if dz or dy]
    offsets.sort(key=lambda o: -(min(o[0], n - o[0]) + min(o[1], n - o[1])))
    for b in range(2):
        for dz, dy in offsets:
            peer = lax.rem(z + dz, n) * n + lax.rem(y + dy, n)
            remote(
                outgoing.at[b, peer],
                incoming.at[b, lax.rem(f, 4), f // 4],
                w_send.at[b],
                w_recv.at[b],
                (peer, t),
            ).start()

        pltpu.make_async_copy(
            outgoing.at[b, f], incoming.at[b, lax.rem(f, 4), f // 4], w_recv.at[b]
        ).start()

    drain(tokens, in_sem.at[2])
    wide = tokens[...].astype(F32)
    normed_rows = rsqrt_norm(wide)
    spot = lax.broadcasted_iota(jnp.int32, (2 * half, 2 * half), 0)
    source = lax.broadcasted_iota(jnp.int32, (2 * half, 2 * half), 1)
    in_first = spot < half
    inside = jnp.where(in_first, spot, spot - half)
    major = inside // block
    minor = (inside % block) // OWN
    row = inside % OWN
    first_home = major * n + 2 * minor + major % 2
    second_home = (2 * minor + (major + 1) % 2) * n + major
    home = jnp.where(in_first, first_home, second_home) * OWN + row
    shuffle = jnp.where(home == source, 1.0, 0.0).astype(BF16)
    normed[...] = jnp.dot(shuffle, normed_rows, preferred_element_type=F32).astype(BF16)
    pick_row = lax.broadcasted_iota(jnp.int32, (8, 2 * half), 0)
    pick_source = lax.broadcasted_iota(jnp.int32, (8, 2 * half), 1)
    pick = jnp.where((pick_row < OWN) & (pick_source == pick_row + f * OWN), 1.0, 0.0).astype(BF16)
    mine = jnp.dot(pick, tokens[...], preferred_element_type=F32)[0:OWN]

    lanes = 3 * 128
    lane_in = lax.broadcasted_iota(jnp.int32, (128, lanes), 0)
    lane_out = lax.broadcasted_iota(jnp.int32, (128, lanes), 1)
    inner = lane_out % 128

    def merge(b):
        drain(incoming.at[b], w_recv.at[b])
        total = jnp.zeros((fs // 4 * ROWS, lanes), F32)
        for i in range(4):
            chosen = (inner // 32 == i) & (lane_in == lane_out // 128 * 32 + inner % 32)
            spread_out = jnp.where(chosen, 1.0, 0.0).astype(BF16)
            piece = incoming[b, i].reshape(fs // 4 * ROWS, 128)
            total = total + jnp.dot(piece, spread_out, preferred_element_type=F32)
        for j in range(fs // 4):
            for w in range(3):
                there = slice(j * 128, (j + 1) * 128)
                cut = total[j * ROWS : (j + 1) * ROWS, w * 128 : (w + 1) * 128]
                weights_8[b, t, w, :, there] = cut[0:8].astype(BF16)
                weights_4[b, t, w, :, there] = cut[8:12].astype(BF16)

    def chunks(s):
        return ((0, 1), (1, 1), (2, 1)) if s == 0 else ((0, 3),)

    def send_piece(s, slot, chunk, send, recv, device, columns=pl.ds(0, d)):
        for held in (weights_8, weights_4):
            source = held.at[s, slot, pl.ds(*chunk), :, columns]
            remote(source, source, send, recv, device).start()

    def taken(sem, rows, columns=d):
        drain(weights_4.at[pl.ds(0, rows), 0, :, :, pl.ds(0, columns)], sem)

    def taken_sets(sem, count):
        drain(weights_4.at[pl.ds(0, 3), pl.ds(0, count)], sem)

    def index(s, i):
        return i if s == 0 else 2 + s

    def spread(s):
        for i, chunk in enumerate(chunks(s)):
            for h, step in enumerate(around):
                send_piece(s, t, chunk, x_send.at[s], near_recv.at[index(s, i), h], along(step))
            send_piece(s, t, chunk, x_send.at[s], die_recv.at[s], partner)

    def relay(s):
        for i, chunk in enumerate(chunks(s)):
            for h, step in enumerate(around):
                slot = slot_of(-step, c)
                taken(near_recv.at[index(s, i), h], chunk[1])
                if nx == 4:
                    send_piece(
                        s, slot, chunk, x_send.at[s], half_recv.at[index(s, i), h], along(step),
                        pl.ds(h * (d // 2), d // 2),
                    )
                send_piece(s, slot, chunk, x_send.at[s], die_recv.at[s], partner)

    def finish(s):
        if nx == 4:
            for i, chunk in enumerate(chunks(s)):
                for h in range(2):
                    taken(half_recv.at[index(s, i), h], chunk[1], d // 2)
                    send_piece(
                        s, slot_of(2, c), chunk, x_send.at[s], die_recv.at[s], partner,
                        pl.ds(h * (d // 2), d // 2),
                    )

    def collected(s):
        taken_sets(die_recv.at[s], nx)

    def units(s, w):
        tail = jnp.concatenate([weights_4[s, j, w].astype(F32) for j in range(n_tp)], axis=0)
        return jnp.concatenate([weights_8[s, :, w].reshape(n_tp * 8, d), tail.astype(BF16)], axis=0)

    def publish(b):
        width = hu * n_tp
        spot = lax.broadcasted_iota(jnp.int32, (width, n_tp * 12), 0)
        source = lax.broadcasted_iota(jnp.int32, (width, n_tp * 12), 1)
        owner_of, unit = spot % n_tp, spot // n_tp
        from_spot = jnp.where(unit < 8, owner_of * 8 + unit, n_tp * 8 + owner_of * 4 + unit - 8)
        swap = jnp.where(source == from_spot, 1.0, 0.0).astype(BF16)
        for w in range(3):
            rows = jnp.dot(swap, units(b, w), preferred_element_type=F32)
            for r in range(hu):
                staged[3 * b + w, r] = rows[r * n_tp : (r + 1) * n_tp].astype(BF16)
            pltpu.make_async_copy(staged.at[3 * b + w], served[3 * b + w], out_sem.at[b]).start()

    contract = (((1,), (1,)), ((), ()))

    def branch_of(rows, gate, up, down):
        gate_act = lax.dot_general(rows, gate, contract, preferred_element_type=F32)
        up_act = lax.dot_general(rows, up, contract, preferred_element_type=F32)
        act = (gate_act / (1.0 + jnp.exp(-gate_act)) * up_act).astype(BF16)
        return jnp.dot(act, down, preferred_element_type=F32).astype(BF16)

    def send_blocks(source, target, me, count, send, recv, device):
        for k in far_first(count):
            peer = lax.rem(me + k, count)
            remote(source.at[peer], target.at[me], send, recv, device(peer)).start()

        pltpu.make_async_copy(source.at[me], target.at[me], recv).start()

    def reduced(target, count, recv):
        drain(target, recv)
        total = target[0].astype(F32)
        for k in range(1, count):
            total = total + target[k].astype(F32)
        return total

    def hand_groups(total, held, targets, me, own, send, recv, device):
        for k, peer in enumerate(targets):
            held[k] = total[k * OWN : (k + 1) * OWN].astype(BF16)

            @pl.when(peer != me)
            def _():
                remote(held.at[k], own.at[me], send, recv, device(peer)).start()

            @pl.when(peer == me)
            def _():
                pltpu.make_async_copy(held.at[k], own.at[me], recv).start()

    def added(own, count):
        total = own[0].astype(F32)
        for k in range(1, count):
            total = total + own[k].astype(F32)
        return total

    merge(0)
    spread(0)
    relay(0)
    merge(1)
    quad = [((z + 1 - 2 * ez) * n + y, t), (z * n + y + 1 - 2 * ey, t)]
    quad.append(((z + 1 - 2 * ez) * n + y + 1 - 2 * ey, t))
    for k, device in enumerate(quad):
        for held in (weights_8, weights_4):
            remote(held.at[1, t], held.at[2 + k, t], quad_send.at[k], quad_recv.at[k], device).start()
    finish(0)
    collected(0)
    block_one = [units(0, w) for w in range(3)]
    for side in range(2):
        rows = normed[side * half : (side + 1) * half, :]
        part[side * n : (side + 1) * n] = branch_of(rows, *block_one).reshape(n, block, d)
        send_blocks(
            part.at[pl.ds(side * n, n)],
            landed.at[side],
            z if side == 0 else y,
            n,
            r_send.at[0],
            r_recv.at[side],
            (lambda peer: at(peer, y)) if side == 0 else (lambda peer: at(z, peer)),
        )
    spread(1)
    publish(0)
    for k in range(3):
        taken(quad_recv.at[k], 3)
        spread(2 + k)
    relay(1)
    relay(2)
    total = reduced(landed.at[0], n, r_recv.at[0])
    hand_groups(
        total, group.at[0], [2 * k + lax.rem(z, 2) for k in range(groups)], y,
        owner, q_send.at[0], q_recv.at[0], lambda peer: at(z, peer),
    )
    total = reduced(landed.at[1], n, r_recv.at[1])
    hand_groups(
        total, group.at[1], [2 * k + lax.rem(y + 1, 2) for k in range(groups)], z,
        owner, q_send.at[0], q_recv.at[0], lambda peer: at(peer, y),
    )
    finish(1)
    relay(3)
    drain(owner, q_recv.at[0])
    middle[...] = (mine + 0.5 * added(owner, n)).astype(BF16)
    mid = middle[...].astype(F32)
    own_slot = jnp.where(even, q // 2, m // 2 + p // 2)
    small[own_slot] = rsqrt_norm(mid)
    for k in far_first(m):
        near, far = at_two(p, lax.rem(q + k, m)), at_two(lax.rem(p + k, m), q)
        peer = jnp.where(even, near[0], far[0])
        remote(small.at[own_slot], small.at[own_slot], s_send, s_recv, (peer, t)).start()
    finish(2)
    relay(4)
    drain(small.at[pl.ds(0, m - 1)], s_recv)
    for side in range(2):
        rows = jnp.concatenate(
            [small[side * (m // 2) + k].astype(F32) for k in range(m // 2)], axis=0
        )
        me = p if side == 0 else q
        gathered[side, me] = rows.astype(BF16)
        for k in far_first(m):
            peer = lax.rem(me + k, m)
            remote(
                gathered.at[side, me], gathered.at[side, me], g_send.at[side], g_recv.at[side],
                at_two(peer, q) if side == 0 else at_two(p, peer),
            ).start()
    finish(3)
    finish(4)
    for s in range(1, 5):
        collected(s)
        for w in range(3):
            ready[w, (s - 1) * 12 * n_tp : s * 12 * n_tp, :] = units(s, w)
    quarter = OWN * m * m // 2
    for side in range(2):
        drain(gathered.at[side, pl.ds(0, m - 1)], g_recv.at[side])
    branch = branch_of(gathered[...].reshape(2 * quarter, d), ready[0], ready[1], ready[2])
    part_two[...] = branch.reshape(part_two.shape)
    for side in range(2):
        send_blocks(
            part_two.at[side], landed_two.at[side], p if side == 0 else q, m, r_send.at[1 + side],
            r_recv.at[2 + side],
            (lambda peer: at_two(peer, q)) if side == 0 else (lambda peer: at_two(p, peer)),
        )
    publish(1)
    total = reduced(landed_two.at[0], m, r_recv.at[2])
    hand_groups(
        total, group_two.at[0], [2 * k + lax.rem(p, 2) for k in range(m // 2)], q,
        owner_two, q_send.at[1], q_recv.at[1], lambda peer: at_two(p, peer),
    )
    total = reduced(landed_two.at[1], m, r_recv.at[3])
    hand_groups(
        total, group_two.at[1], [2 * k + lax.rem(q + 1, 2) for k in range(m // 2)], p,
        owner_two, q_send.at[1], q_recv.at[1], lambda peer: at_two(peer, q),
    )
    for k in range(3):
        taken(quad_send.at[k], 3)
    for s in range(5):
        taken_sets(x_send.at[s], 2 * nx - 1)
    drain(small.at[pl.ds(0, m - 1)], s_send)
    drain(part_two.at[0].at[pl.ds(0, m - 1)], g_send.at[0])
    drain(part_two.at[0].at[pl.ds(0, m - 1)], g_send.at[1])
    drain(part.at[pl.ds(0, 2 * n - 2)], r_send.at[0])
    drain(owner.at[pl.ds(0, n - 1)], q_send.at[0])
    for b in range(2):
        drain(outgoing.at[b, pl.ds(0, fs - 1)], w_send.at[b])
        drain(staged.at[pl.ds(3 * b, 3)], out_sem.at[b])
        drain(part_two.at[0].at[pl.ds(0, m - 1)], r_send.at[1 + b])
    drain(owner_two.at[pl.ds(0, m - 1)], q_send.at[1])
    drain(owner_two, q_recv.at[1])
    mixed[...] = (mid + 0.5 * added(owner_two, m)).astype(BF16)


def deliver(count, *refs):
    sources, targets, held = refs[:count], refs[count : 2 * count], refs[2 * count : 3 * count]
    in_sem, out_sem = refs[3 * count :]
    taken = [pltpu.make_async_copy(sources[k], held[k], in_sem.at[k]) for k in range(count)]
    given = [pltpu.make_async_copy(held[k], targets[k], out_sem.at[k]) for k in range(count)]
    for copy in taken:
        copy.start()
    for k in range(count):
        taken[k].wait()
        given[k].start()
    for copy in given:
        copy.wait()


def shards(
    tokens, gain_first, gate_first, up_first, down_first, gain_second, gate_second, up_second, down_second
):
    fs, n_tp = lax.axis_size("fs"), lax.axis_size("tp")
    n = int(round(fs**0.5))
    fd, local = gate_first.shape
    hu = local // fs
    d = fs * fd
    rows = tokens.shape[1]
    block = rows // 2 // n
    wide = -(-(local + ROWS) // 128) * 128
    vmem = pl.BlockSpec(memory_space=pltpu.VMEM)
    hbm = pl.BlockSpec(memory_space=pltpu.HBM)
    dma = pltpu.SemaphoreType.DMA
    m = n // 2
    two = (2, m, OWN * m // 2, d)
    results = pl.pallas_call(
        functools.partial(kernel, n, n_tp, hu, fd),
        out_shape=(
            jax.ShapeDtypeStruct((OWN, d), BF16),
        )
        + (jax.ShapeDtypeStruct((hu, n_tp, d), BF16),) * 6,
        in_specs=[hbm] * 9,
        out_specs=(vmem,) + (hbm,) * 6,
        scratch_shapes=[
            pltpu.VMEM((rows, d), BF16),
            pltpu.VMEM((2, 1, fd), F32),
            pltpu.VMEM((2, 3, fd, local), F32),
            pltpu.VMEM((4 * fd, wide), F32),
            pltpu.VMEM((wide, 4 * fd), F32),
            pltpu.VMEM((2, fs, ROWS, 128), BF16),
            pltpu.VMEM((2, 4, fs // 4, ROWS, 128), BF16),
            pltpu.VMEM((5, n_tp, 3, 8, d), BF16),
            pltpu.VMEM((5, n_tp, 3, 4, d), BF16),
            pltpu.VMEM((3, 4 * 12 * n_tp, d), BF16),
            pltpu.VMEM((rows, d), BF16),
            pltpu.VMEM((2 * n, block, d), BF16),
            pltpu.VMEM((2, n, block, d), BF16),
            pltpu.VMEM((2, m, OWN, d), BF16),
            pltpu.VMEM((n, OWN, d), BF16),
            pltpu.VMEM((m, OWN, d), BF16),
            pltpu.VMEM(two, BF16),
            pltpu.VMEM(two, BF16),
            pltpu.VMEM(two, BF16),
            pltpu.VMEM((2, m // 2, OWN, d), BF16),
            pltpu.VMEM((m, OWN, d), BF16),
            pltpu.VMEM((OWN, d), BF16),
            pltpu.VMEM((6, hu, n_tp, d), BF16),
            dma((2,)), dma((2,)), dma((5,)), dma((7, 2)), dma((7, 2)), dma((5,)), dma((3,)), dma((3,)),
            dma((3,)), dma((4,)), dma((2,)), dma((2,)), dma(()), dma(()), dma((2,)), dma((2,)),
            dma((4,)), dma((2,)),
        ],
        compiler_params=pltpu.CompilerParams(
            collective_id=0, has_side_effects=True, vmem_limit_bytes=67043328
        ),
    )(
        tokens[0],
        gain_first[None], gate_first, up_first, down_first,
        gain_second[None], gate_second, up_second, down_second,
    )
    mixed, *served = pl.pallas_call(
        functools.partial(deliver, 7),
        out_shape=tuple(jax.ShapeDtypeStruct(r.shape, r.dtype) for r in results),
        in_specs=[hbm] * 7,
        out_specs=(hbm,) * 7,
        scratch_shapes=[pltpu.VMEM(r.shape, r.dtype) for r in results] + [dma((7,)), dma((7,))],
    )(*results)
    return (mixed[None],) + tuple(jnp.swapaxes(r, 0, 1) for r in served)


def solution(mesh):
    weight = P("fs", "tp")
    cut = P(None, "fs", None)
    return jax.shard_map(
        shards,
        mesh=mesh,
        in_specs=(P("tp", None, None), P("fs"), weight, weight, weight, P("fs"), weight, weight, weight),
        out_specs=(P("tp", "fs", None),) + (cut,) * 6,
        check_vma=False,
    )
```

time: 88.3 us -> 83.3 us (0.943)
  Pallas kernels: 87.4 us -> 82.5 us
    pallas_call x1, Pallas kernels: 85 us -> 80 us  [shards(): pl.pallas_call(functools.partial(kernel, n, n_tp, hu, fd), out_shape=(jax...]
where the time goes in v5:
time: 83.3 us; the launch traced here: 83.1 us
  Pallas kernels  82.5 us (99%)
    pallas_call x1, Pallas kernels, shards(): pl.pallas_call(functools.partial(kernel, n, n_tp, hu, fd), out_shape=(jax...  80 us
    pallas_call x1, Pallas kernels, shards(): pl.pallas_call(functools.partial(deliver, 7), out_shape=tuple((jax.ShapeD...  2.45 us

profile of v5, /device:TPU:1, one launch (start us, length us, event | category | flops | bytes accessed | tf_op | source)
XLA Modules:
  0.0 83.1 jit_solution(1634120988868792969)
XLA Ops:
  0.6 80.0 %shard_map.144 = (bf16[4,2048]{1,0:T(4,128)(2,1)}, bf16[11,8,2048]{2,1,0:T(8,128)(2,1)}, bf16[11,8,2048]{2,1,0:T(8,128)(2,1)}, bf16[11,8,2048]{2,1,0:T(8,128)(2,...) custom-call(bf16[256,2048]{1,0:T(8,128)(2,1)} %bitcast.10, ...), custom_call_target="tpu_custom_call" | custom-call | tf_op jit(solution)/shard_map/pallas_call | solution.py:410
  80.7 2.5 %shard_map.145 = (bf16[4,2048]{1,0:T(4,128)(2,1)}, bf16[11,8,2048]{2,1,0:T(8,128)(2,1)}, bf16[11,8,2048]{2,1,0:T(8,128)(2,1)}, bf16[11,8,2048]{2,1,0:T(8,128)(2,...) custom-call(bf16[4,2048]{1,0:T(4,128)(2,1)} %get-tuple-element.21.refs_0_, ...), custom_call_target="tpu_custom_call" | custom-call | tf_op jit(solution)/shard_map/pallas_call | solution.py:454

commit v6 on v5

v6 whole, which is shorter than its diff:
```python
import functools

import jax
import jax.numpy as jnp
from jax import lax
from jax.experimental import pallas as pl
from jax.experimental.pallas import tpu as pltpu
from jax.sharding import PartitionSpec as P

MESH = pl.DeviceIdType.MESH
F32, BF16 = jnp.float32, jnp.bfloat16
SENT = 12
OWN = 4


def far_first(count):
    return sorted(range(1, count), key=lambda k: (-min(k, count - k), k))


def rsqrt_norm(wide):
    scale = lax.rsqrt(jnp.mean(wide * wide, axis=-1, keepdims=True) + 1e-06)
    return (wide * scale).astype(BF16)


def kernel(
    n, n_tp, hu, fd,
    tokens_hbm, gain_one, gate_one, up_one, down_one, gain_two, gate_two, up_two, down_two,
    mixed, out_0, out_1, out_2, out_3, out_4, out_5,
    tokens, gains, trained, stack, turned, outgoing, incoming, placing, weights_8, weights_4, ready, normed,
    part, landed, group, line, gathered, part_two, landed_two, group_two, owner_two, middle, residual, staged,
    w_send, w_recv, x_send, near_recv, half_recv, die_recv, quad_send, quad_recv, r_send, r_recv,
    l_send, l_recv, two_send, two_recv, q_send, q_recv, g_send, g_recv, in_sem, out_sem,
):
    served = (out_0, out_1, out_2, out_3, out_4, out_5)
    fs = n * n
    d = fs * fd
    half = OWN * fs // 2
    block = half // n
    m = n // 2
    share = OWN * m // 2
    f, t = lax.axis_index("fs"), lax.axis_index("tp")
    z, y = f // n, lax.rem(f, n)
    ez, ey, p, q = lax.rem(z, 2), lax.rem(y, 2), z // 2, y // 2
    x, c = t // 2, lax.rem(t, 2)
    nx = n_tp // 2
    even = lax.rem(p + q, 2) == 0
    partner = (f, x * 2 + 1 - c)

    def at(zz, yy):
        return (zz * n + yy, t)

    def at_two(pp, qq):
        return ((2 * pp + ez) * n + 2 * qq + ey, t)

    def along(step):
        return (f, lax.rem(x + nx + step, nx) * 2 + c)

    def slot_of(step, core):
        return lax.rem(x + nx + step, nx) * 2 + core

    def remote(src, dst, send, recv, device):
        return pltpu.make_async_remote_copy(
            src_ref=src, dst_ref=dst, send_sem=send, recv_sem=recv, device_id=device, device_id_type=MESH
        )

    def drain(ref, sem):
        pltpu.make_async_copy(ref, ref, sem).wait()

    given = ((gain_one, gate_one, up_one, down_one), (gain_two, gate_two, up_two, down_two))
    for b, (gain, *each) in enumerate(given):
        pltpu.make_async_copy(gain, gains.at[b], in_sem.at[3]).start()
        for w in range(3):
            pltpu.make_async_copy(each[w], trained.at[b, w], in_sem.at[b]).start()
    pltpu.make_async_copy(tokens_hbm, tokens, in_sem.at[2]).start()

    barrier = pltpu.get_barrier_semaphore()

    @pl.loop(1, fs)
    def _(k):
        pl.semaphore_signal(barrier, inc=1, device_id=(lax.rem(f + k, fs), t), device_id_type=MESH)

    around = {1: (), 2: (1,), 4: (1, -1)}[nx]
    for step in around:
        pl.semaphore_signal(barrier, inc=1, device_id=along(step), device_id_type=MESH)
    pl.semaphore_signal(barrier, inc=1, device_id=partner, device_id_type=MESH)

    hidden_units = gate_one.shape[1]
    stack[...] = jnp.zeros_like(stack)
    drain(gains, in_sem.at[3])
    for b in range(2):
        drain(trained.at[b], in_sem.at[b])
        for w in range(3):
            stack[w * fd : (w + 1) * fd, 0:hidden_units] = trained[b, w]
        ones = jnp.ones((1, fd), F32)
        scale = jnp.concatenate([gains[b], gains[b], ones, ones], axis=1)
        turned[...] = stack[...].T * scale
        live = lax.broadcasted_iota(jnp.int32, (SENT, 128), 0) < hu
        for k in range(fs):
            rows = jnp.where(live, turned[k * hu : k * hu + SENT, :], 0.0)
            for g in range(SENT // 4):
                outgoing[b, k, g] = rows[4 * g : 4 * g + 4].astype(BF16)

    lanes = 3 * 128
    lane_in = lax.broadcasted_iota(jnp.int32, (128, lanes), 0)
    lane_out = lax.broadcasted_iota(jnp.int32, (128, lanes), 1)
    inner = lane_out % 128
    for i in range(4):
        chosen = (inner // 32 == i) & (lane_in == lane_out // 128 * 32 + inner % 32)
        placing[i] = jnp.where(chosen, 1.0, 0.0).astype(BF16)

    pl.semaphore_wait(barrier, fs - 1 + len(around) + 1)

    offsets = [(dz, dy) for dz in range(n) for dy in range(n) if dz or dy]
    offsets.sort(key=lambda o: (min(o[0], n - o[0]), -min(o[1], n - o[1])))
    for b in range(2):
        for dz, dy in offsets:
            peer = lax.rem(z + dz, n) * n + lax.rem(y + dy, n)
            remote(
                outgoing.at[b, peer],
                incoming.at[b, lax.rem(f, 4), f // 4],
                w_send.at[b],
                w_recv.at[z if b == 0 else n],
                (peer, t),
            ).start()

        pltpu.make_async_copy(
            outgoing.at[b, f], incoming.at[b, lax.rem(f, 4), f // 4], w_recv.at[z if b == 0 else n]
        ).start()

    drain(tokens, in_sem.at[2])
    wide = tokens[...].astype(F32)
    normed_rows = rsqrt_norm(wide)
    spot = lax.broadcasted_iota(jnp.int32, (2 * half, 2 * half), 0)
    source = lax.broadcasted_iota(jnp.int32, (2 * half, 2 * half), 1)
    in_first = spot < half
    inside = jnp.where(in_first, spot, spot - half)
    major = inside // block
    side_e = inside % block // share
    minor = inside % share // OWN
    row = inside % OWN
    first_home = major * n + 2 * (2 * minor + major // 2 % 2) + side_e
    second_home = (2 * (2 * minor + (major // 2 + 1) % 2) + side_e) * n + major
    home = jnp.where(in_first, first_home, second_home) * OWN + row
    shuffle = jnp.where(home == source, 1.0, 0.0).astype(BF16)
    normed[...] = jnp.dot(shuffle, normed_rows, preferred_element_type=F32).astype(BF16)
    pick_row = lax.broadcasted_iota(jnp.int32, (2 * share, 2 * half), 0)
    pick_source = lax.broadcasted_iota(jnp.int32, (2 * share, 2 * half), 1)
    inside = pick_row % share
    row_home = jnp.where(
        pick_row < share,
        z * n + 2 * (2 * (inside // OWN) + lax.rem(p, 2)) + ey,
        (2 * (2 * (inside // OWN) + lax.rem(q + 1, 2)) + ez) * n + y,
    )
    pick = jnp.where(pick_source == row_home * OWN + inside % OWN, 1.0, 0.0).astype(BF16)
    residual[...] = jnp.dot(pick, tokens[...], preferred_element_type=F32)

    per = n // 4
    strip = n * fd

    def merge(b, first, count, start):
        total = jnp.zeros((count * SENT, lanes), F32)
        for i in range(4):
            rows = jnp.concatenate(
                [incoming[b, i, first + j, g].astype(F32) for j in range(count) for g in range(SENT // 4)],
                axis=0,
            )
            total = total + jnp.dot(rows.astype(BF16), placing[i], preferred_element_type=F32)
        for j in range(count):
            for w in range(3):
                there = pl.ds(start + j * 128, 128)
                cut = total[j * SENT : (j + 1) * SENT, w * 128 : (w + 1) * 128]
                weights_8[b, t, w, :, there] = cut[0:8].astype(BF16)
                weights_4[b, t, w, :, there] = cut[8:12].astype(BF16)

    def send_piece(s, slot, send, recv, device, columns=pl.ds(0, d)):
        for held in (weights_8, weights_4):
            source = held.at[s, slot, :, :, columns]
            remote(source, source, send, recv, device).start()

    def taken(sem, columns=d):
        drain(weights_4.at[pl.ds(0, 3), 0, :, :, pl.ds(0, columns)], sem)

    def taken_sets(sem, count):
        drain(weights_4.at[pl.ds(0, 3), pl.ds(0, count)], sem)

    near_first = [0] + far_first(n)[::-1]

    def columns_of(u):
        return pl.multiple_of(lax.rem(z + near_first[u], n) * strip, strip)

    def stream(u):
        home = lax.rem(z + near_first[u], n)
        drain(incoming.at[0, 0, pl.ds(0, n)], w_recv.at[home])
        merge(0, home * per, per, columns_of(u))
        columns = pl.ds(columns_of(u), strip)
        for h, step in enumerate(around):
            send_piece(0, t, x_send.at[0], near_recv.at[u, h], along(step), columns)
        send_piece(0, t, x_send.at[0], die_recv.at[0], partner, columns)

    def stream_relay(u):
        columns = pl.ds(columns_of(u), strip)
        for h, step in enumerate(around):
            slot = slot_of(-step, c)
            taken(near_recv.at[u, h], strip)
            if nx == 4 and h == u % 2:
                send_piece(0, slot, x_send.at[0], half_recv.at[u], along(step), columns)
            send_piece(0, slot, x_send.at[0], die_recv.at[0], partner, columns)

    def stream_finish(u):
        if nx == 4:
            taken(half_recv.at[u], strip)
            send_piece(
                0, slot_of(2, c), x_send.at[0], die_recv.at[0], partner, pl.ds(columns_of(u), strip)
            )

    def spread(s):
        for h, step in enumerate(around):
            send_piece(s, t, x_send.at[s], near_recv.at[n + s - 1, h], along(step))
        send_piece(s, t, x_send.at[s], die_recv.at[s], partner)

    def relay(s):
        for h, step in enumerate(around):
            slot = slot_of(-step, c)
            taken(near_recv.at[n + s - 1, h])
            if nx == 4:
                send_piece(
                    s, slot, x_send.at[s], half_recv.at[n + 2 * (s - 1) + h], along(step),
                    pl.ds(h * (d // 2), d // 2),
                )
            send_piece(s, slot, x_send.at[s], die_recv.at[s], partner)

    def finish(s):
        if nx == 4:
            for h in range(2):
                taken(half_recv.at[n + 2 * (s - 1) + h], d // 2)
                send_piece(
                    s, slot_of(2, c), x_send.at[s], die_recv.at[s], partner, pl.ds(h * (d // 2), d // 2)
                )

    def collected(s):
        taken_sets(die_recv.at[s], nx)

    def units(s, w):
        tail = jnp.concatenate([weights_4[s, j, w].astype(F32) for j in range(n_tp)], axis=0)
        return jnp.concatenate([weights_8[s, :, w].reshape(n_tp * 8, d), tail.astype(BF16)], axis=0)

    def publish(b):
        width = hu * n_tp
        spot = lax.broadcasted_iota(jnp.int32, (width, n_tp * 12), 0)
        source = lax.broadcasted_iota(jnp.int32, (width, n_tp * 12), 1)
        owner_of, unit = spot % n_tp, spot // n_tp
        from_spot = jnp.where(unit < 8, owner_of * 8 + unit, n_tp * 8 + owner_of * 4 + unit - 8)
        swap = jnp.where(source == from_spot, 1.0, 0.0).astype(BF16)
        for w in range(3):
            rows = jnp.dot(swap, units(b, w), preferred_element_type=F32)
            for r in range(hu):
                staged[3 * b + w, r] = rows[r * n_tp : (r + 1) * n_tp].astype(BF16)
            pltpu.make_async_copy(staged.at[3 * b + w], served[3 * b + w], out_sem.at[b]).start()

    contract = (((1,), (1,)), ((), ()))

    def hidden_of(rows, gate, up):
        gate_act = lax.dot_general(rows, gate, contract, preferred_element_type=F32)
        up_act = lax.dot_general(rows, up, contract, preferred_element_type=F32)
        return (gate_act / (1.0 + jnp.exp(-gate_act)) * up_act).astype(BF16)

    def branch_of(hidden, down):
        return jnp.dot(hidden, down, preferred_element_type=F32).astype(BF16)

    def send_blocks(source, target, me, count, send, recv, device):
        for k in far_first(count):
            peer = lax.rem(me + k, count)
            remote(source.at[peer], target.at[me], send, recv, device(peer)).start()

        pltpu.make_async_copy(source.at[me], target.at[me], recv).start()

    def reduced(target, count, recv):
        drain(target, recv)
        total = target[0].astype(F32)
        for k in range(1, count):
            total = total + target[k].astype(F32)
        return total

    def hand_groups(total, held, targets, me, own, send, recv, device):
        for k, peer in enumerate(targets):
            held[k] = total[k * OWN : (k + 1) * OWN].astype(BF16)

            @pl.when(peer != me)
            def _():
                remote(held.at[k], own.at[me], send, recv, device(peer)).start()

            @pl.when(peer == me)
            def _():
                pltpu.make_async_copy(held.at[k], own.at[me], recv).start()

    def added(own, count):
        total = own[0].astype(F32)
        for k in range(1, count):
            total = total + own[k].astype(F32)
        return total

    for u in range(n + 6):
        if u < n:
            stream(u)
        if 3 <= u < n + 3:
            stream_relay(u - 3)
        if 6 <= u:
            if u == n + 4:
                break
            stream_finish(u - 6)
    drain(incoming.at[1], w_recv.at[n])
    merge(1, 0, fs // 4, 0)
    quad = [((z + 1 - 2 * ez) * n + y, t), (z * n + y + 1 - 2 * ey, t)]
    quad.append(((z + 1 - 2 * ez) * n + y + 1 - 2 * ey, t))
    for k, device in enumerate(quad):
        for held in (weights_8, weights_4):
            remote(held.at[1, t], held.at[2 + k, t], quad_send.at[k], quad_recv.at[k], device).start()
    spread(1)
    stream_finish(n - 2)
    stream_finish(n - 1)
    collected(0)
    hidden = hidden_of(normed[...], units(0, 0), units(0, 1))
    down_one = units(0, 2)
    wide = d // 2
    for cut in range(2):
        columns = slice(cut * wide, (cut + 1) * wide)
        for side in range(2):
            branch = branch_of(hidden[side * half : (side + 1) * half], down_one[:, columns])
            part[side, :, :, columns] = branch.reshape(n, block, wide)
            me = z if side == 0 else y
            for k in far_first(n):
                peer = lax.rem(me + k, n)
                remote(
                    part.at[side, peer, :, columns], landed.at[side, me, :, columns],
                    r_send.at[side], r_recv.at[side, cut], at(peer, y) if side == 0 else at(z, peer),
                ).start()
            pltpu.make_async_copy(
                part.at[side, me, :, columns], landed.at[side, me, :, columns], r_recv.at[side, cut]
            ).start()

    def sum_cut(cut):
        columns = slice(cut * wide, (cut + 1) * wide)
        for side in range(2):
            drain(landed.at[side, :, :, columns], r_recv.at[side, cut])
            total = landed[side, 0, :, columns].astype(F32)
            for k in range(1, n):
                total = total + landed[side, k, :, columns].astype(F32)
            for k in range(2):
                group[side, k, :, columns] = total[k * share : (k + 1) * share].astype(BF16)
            me = y if side == 0 else z
            for k in far_first(n):
                peer = lax.rem(me + k, n)
                remote(
                    group.at[side, lax.rem(peer, 2), :, columns], line.at[side, me, :, columns],
                    l_send.at[side], l_recv.at[side], at(z, peer) if side == 0 else at(peer, y),
                ).start()
            pltpu.make_async_copy(
                group.at[side, lax.rem(me, 2), :, columns], line.at[side, me, :, columns], l_recv.at[side]
            ).start()

    def prepare(s):
        collected(s)
        for w in range(3):
            ready[w, (s - 1) * SENT * n_tp : s * SENT * n_tp, :] = units(s, w)

    taken(quad_recv.at[0])
    spread(2)
    relay(1)
    for k in range(1, 3):
        taken(quad_recv.at[k])
        spread(2 + k)
    publish(0)
    sum_cut(0)
    relay(2)
    sum_cut(1)
    finish(1)
    relay(3)
    prepare(1)
    own_slot = jnp.where(even, q // 2, m // 2 + p // 2)
    for side in range(2):
        drain(line.at[side], l_recv.at[side])
        total = line[side, 0].astype(F32)
        for k in range(1, n):
            total = total + line[side, k].astype(F32)
        total = residual[side * share : (side + 1) * share] + 0.5 * total
        for k in range(m // 2):
            middle[side * (m // 2) + k] = total[k * OWN : (k + 1) * OWN].astype(BF16)
        me = p if side == 0 else q
        gathered[side, me] = rsqrt_norm(total.astype(BF16).astype(F32))
        for k in far_first(m):
            peer = lax.rem(me + k, m)
            remote(
                gathered.at[side, me], gathered.at[side, me], g_send.at[side], g_recv.at[side],
                at_two(peer, q) if side == 0 else at_two(p, peer),
            ).start()
    finish(2)
    relay(4)
    prepare(2)
    finish(3)
    prepare(3)
    finish(4)
    prepare(4)
    quarter = OWN * m * m // 2
    for side in range(2):
        drain(gathered.at[side, pl.ds(0, m - 1)], g_recv.at[side])
    hidden = hidden_of(gathered[...].reshape(2 * quarter, d), ready[0], ready[1])
    branch = branch_of(hidden, ready[2])
    part_two[...] = branch.reshape(part_two.shape)
    for side in range(2):
        send_blocks(
            part_two.at[side], landed_two.at[side], p if side == 0 else q, m, two_send.at[side],
            two_recv.at[side],
            (lambda peer: at_two(peer, q)) if side == 0 else (lambda peer: at_two(p, peer)),
        )
    publish(1)
    total = reduced(landed_two.at[0], m, two_recv.at[0])
    hand_groups(
        total, group_two.at[0], [2 * k + lax.rem(p, 2) for k in range(m // 2)], q,
        owner_two, q_send, q_recv, lambda peer: at_two(p, peer),
    )
    total = reduced(landed_two.at[1], m, two_recv.at[1])
    hand_groups(
        total, group_two.at[1], [2 * k + lax.rem(q + 1, 2) for k in range(m // 2)], p,
        owner_two, q_send, q_recv, lambda peer: at_two(peer, q),
    )
    for k in range(3):
        taken(quad_send.at[k])
    for s in range(5):
        taken_sets(x_send.at[s], 2 * nx - 1)
    for b in range(2):
        drain(outgoing.at[b, pl.ds(0, fs - 1)], w_send.at[b])
        drain(staged.at[pl.ds(3 * b, 3)], out_sem.at[b])
        drain(part.at[b, pl.ds(0, n - 1)], r_send.at[b])
        drain(line.at[b, pl.ds(0, n - 1)], l_send.at[b])
        drain(gathered.at[b, pl.ds(0, m - 1)], g_send.at[b])
        drain(gathered.at[b, pl.ds(0, m - 1)], two_send.at[b])
    drain(owner_two.at[pl.ds(0, m - 1)], q_send)
    drain(owner_two, q_recv)
    mixed[...] = (middle[own_slot].astype(F32) + 0.5 * added(owner_two, m)).astype(BF16)


def deliver(count, *refs):
    sources, targets, held = refs[:count], refs[count : 2 * count], refs[2 * count : 3 * count]
    in_sem, out_sem = refs[3 * count :]
    taken = [pltpu.make_async_copy(sources[k], held[k], in_sem.at[k]) for k in range(count)]
    given = [pltpu.make_async_copy(held[k], targets[k], out_sem.at[k]) for k in range(count)]
    for copy in taken:
        copy.start()
    for k in range(count):
        taken[k].wait()
        given[k].start()
    for copy in given:
        copy.wait()


def shards(
    tokens, gain_first, gate_first, up_first, down_first, gain_second, gate_second, up_second, down_second
):
    fs, n_tp = lax.axis_size("fs"), lax.axis_size("tp")
    n = int(round(fs**0.5))
    fd, local = gate_first.shape
    hu = local // fs
    d = fs * fd
    rows = tokens.shape[1]
    block = rows // 2 // n
    wide = -(-(local + 16) // 128) * 128
    vmem = pl.BlockSpec(memory_space=pltpu.VMEM)
    hbm = pl.BlockSpec(memory_space=pltpu.HBM)
    dma = pltpu.SemaphoreType.DMA
    m = n // 2
    two = (2, m, OWN * m // 2, d)
    results = pl.pallas_call(
        functools.partial(kernel, n, n_tp, hu, fd),
        out_shape=(
            jax.ShapeDtypeStruct((OWN, d), BF16),
        )
        + (jax.ShapeDtypeStruct((hu, n_tp, d), BF16),) * 6,
        in_specs=[hbm] * 9,
        out_specs=(vmem,) + (hbm,) * 6,
        scratch_shapes=[
            pltpu.VMEM((rows, d), BF16),
            pltpu.VMEM((2, 1, fd), F32),
            pltpu.VMEM((2, 3, fd, local), F32),
            pltpu.VMEM((4 * fd, wide), F32),
            pltpu.VMEM((wide, 4 * fd), F32),
            pltpu.VMEM((2, fs, SENT // 4, 4, 128), BF16),
            pltpu.VMEM((2, 4, fs // 4, SENT // 4, 4, 128), BF16),
            pltpu.VMEM((4, 128, 3 * 128), BF16),
            pltpu.VMEM((5, n_tp, 3, 8, d), BF16),
            pltpu.VMEM((5, n_tp, 3, 4, d), BF16),
            pltpu.VMEM((3, 4 * 12 * n_tp, d), BF16),
            pltpu.VMEM((rows, d), BF16),
            pltpu.VMEM((2, n, block, d), BF16),
            pltpu.VMEM((2, n, block, d), BF16),
            pltpu.VMEM((2, 2, OWN * m // 2, d), BF16),
            pltpu.VMEM((2, n, OWN * m // 2, d), BF16),
            pltpu.VMEM(two, BF16),
            pltpu.VMEM(two, BF16),
            pltpu.VMEM(two, BF16),
            pltpu.VMEM((2, m // 2, OWN, d), BF16),
            pltpu.VMEM((m, OWN, d), BF16),
            pltpu.VMEM((m, OWN, d), BF16),
            pltpu.VMEM((OWN * m, d), F32),
            pltpu.VMEM((6, hu, n_tp, d), BF16),
            dma((2,)), dma((n + 1,)), dma((5,)), dma((n + 4, 2)), dma((n + 8,)), dma((5,)), dma((3,)), dma((3,)),
            dma((2,)), dma((2, 2)), dma((2,)), dma((2,)), dma((2,)), dma((2,)), dma(()), dma(()),
            dma((2,)), dma((2,)), dma((4,)), dma((2,)),
        ],
        compiler_params=pltpu.CompilerParams(
            collective_id=0, has_side_effects=True, vmem_limit_bytes=67043328
        ),
    )(
        tokens[0],
        gain_first[None], gate_first, up_first, down_first,
        gain_second[None], gate_second, up_second, down_second,
    )
    mixed, *served = pl.pallas_call(
        functools.partial(deliver, 7),
        out_shape=tuple(jax.ShapeDtypeStruct(r.shape, r.dtype) for r in results),
        in_specs=[hbm] * 7,
        out_specs=(hbm,) * 7,
        scratch_shapes=[pltpu.VMEM(r.shape, r.dtype) for r in results] + [dma((7,)), dma((7,))],
    )(*results)
    return (mixed[None],) + tuple(jnp.swapaxes(r, 0, 1) for r in served)


def solution(mesh):
    weight = P("fs", "tp")
    cut = P(None, "fs", None)
    return jax.shard_map(
        shards,
        mesh=mesh,
        in_specs=(P("tp", None, None), P("fs"), weight, weight, weight, P("fs"), weight, weight, weight),
        out_specs=(P("tp", "fs", None),) + (cut,) * 6,
        check_vma=False,
    )
```

time: 83.3 us -> 79.7 us (0.957)
  Pallas kernels: 82.5 us -> 78.9 us
    pallas_call x1, Pallas kernels: 80 us -> 76.4 us  [shards(): pl.pallas_call(functools.partial(kernel, n, n_tp, hu, fd), out_shape=(jax...]
where the time goes in v6:
time: 79.7 us; the launch traced here: 79.5 us
  Pallas kernels  78.9 us (99%)
    pallas_call x1, Pallas kernels, shards(): pl.pallas_call(functools.partial(kernel, n, n_tp, hu, fd), out_shape=(jax...  76.4 us
    pallas_call x1, Pallas kernels, shards(): pl.pallas_call(functools.partial(deliver, 7), out_shape=tuple((jax.ShapeD...  2.45 us

profile of v6, /device:TPU:1, one launch (start us, length us, event | category | flops | bytes accessed | tf_op | source)
XLA Modules:
  0.0 79.5 jit_solution(5558132065151031539)
XLA Ops:
  0.6 76.4 %shard_map.144 = (bf16[4,2048]{1,0:T(4,128)(2,1)}, bf16[11,8,2048]{2,1,0:T(8,128)(2,1)}, bf16[11,8,2048]{2,1,0:T(8,128)(2,1)}, bf16[11,8,2048]{2,1,0:T(8,128)(2,...) custom-call(bf16[256,2048]{1,0:T(8,128)(2,1)} %bitcast.10, ...), custom_call_target="tpu_custom_call" | custom-call | tf_op jit(solution)/shard_map/pallas_call | solution.py:472
  77.0 2.5 %shard_map.145 = (bf16[4,2048]{1,0:T(4,128)(2,1)}, bf16[11,8,2048]{2,1,0:T(8,128)(2,1)}, bf16[11,8,2048]{2,1,0:T(8,128)(2,1)}, bf16[11,8,2048]{2,1,0:T(8,128)(2,...) custom-call(bf16[4,2048]{1,0:T(4,128)(2,1)} %get-tuple-element.21.refs_0_, ...), custom_call_target="tpu_custom_call" | custom-call | tf_op jit(solution)/shard_map/pallas_call | solution.py:517

commit v7 on v6

--- a/solution.py
+++ b/solution.py
@@ -27,11 +27,11 @@
     tokens_hbm, gain_one, gate_one, up_one, down_one, gain_two, gate_two, up_two, down_two,
     mixed, out_0, out_1, out_2, out_3, out_4, out_5,
     tokens, gains, trained, stack, turned, outgoing, incoming, placing, weights_8, weights_4, ready, normed,
-    part, landed, group, line, gathered, part_two, landed_two, group_two, owner_two, middle, residual, staged,
+    part, landed, group, line, gathered, part_two, landed_two, group_two, owner_two, middle, residual,
     w_send, w_recv, x_send, near_recv, half_recv, die_recv, quad_send, quad_recv, r_send, r_recv,
-    l_send, l_recv, two_send, two_recv, q_send, q_recv, g_send, g_recv, in_sem, out_sem,
+    l_send, l_recv, two_send, two_recv, q_send, q_recv, g_send, g_recv, in_sem,
 ):
-    served = (out_0, out_1, out_2, out_3, out_4, out_5)
+    staged = (out_0, out_1, out_2, out_3, out_4, out_5)
     fs = n * n
     d = fs * fd
     half = OWN * fs // 2
@@ -254,8 +254,7 @@
         for w in range(3):
             rows = jnp.dot(swap, units(b, w), preferred_element_type=F32)
             for r in range(hu):
-                staged[3 * b + w, r] = rows[r * n_tp : (r + 1) * n_tp].astype(BF16)
-            pltpu.make_async_copy(staged.at[3 * b + w], served[3 * b + w], out_sem.at[b]).start()
+                staged[3 * b + w][r] = rows[r * n_tp : (r + 1) * n_tp].astype(BF16)
 
     contract = (((1,), (1,)), ((), ()))
 
@@ -429,7 +428,6 @@
         taken_sets(x_send.at[s], 2 * nx - 1)
     for b in range(2):
         drain(outgoing.at[b, pl.ds(0, fs - 1)], w_send.at[b])
-        drain(staged.at[pl.ds(3 * b, 3)], out_sem.at[b])
         drain(part.at[b, pl.ds(0, n - 1)], r_send.at[b])
         drain(line.at[b, pl.ds(0, n - 1)], l_send.at[b])
         drain(gathered.at[b, pl.ds(0, m - 1)], g_send.at[b])
@@ -440,16 +438,10 @@
 
 
 def deliver(count, *refs):
-    sources, targets, held = refs[:count], refs[count : 2 * count], refs[2 * count : 3 * count]
-    in_sem, out_sem = refs[3 * count :]
-    taken = [pltpu.make_async_copy(sources[k], held[k], in_sem.at[k]) for k in range(count)]
-    given = [pltpu.make_async_copy(held[k], targets[k], out_sem.at[k]) for k in range(count)]
-    for copy in taken:
+    copies = [pltpu.make_async_copy(refs[k], refs[count + k], refs[-1].at[k]) for k in range(count)]
+    for copy in copies:
         copy.start()
-    for k in range(count):
-        taken[k].wait()
-        given[k].start()
-    for copy in given:
+    for copy in copies:
         copy.wait()
 
 
@@ -476,7 +468,7 @@
         )
         + (jax.ShapeDtypeStruct((hu, n_tp, d), BF16),) * 6,
         in_specs=[hbm] * 9,
-        out_specs=(vmem,) + (hbm,) * 6,
+        out_specs=(vmem,) * 7,
         scratch_shapes=[
             pltpu.VMEM((rows, d), BF16),
             pltpu.VMEM((2, 1, fd), F32),
@@ -501,25 +493,28 @@
             pltpu.VMEM((m, OWN, d), BF16),
             pltpu.VMEM((m, OWN, d), BF16),
             pltpu.VMEM((OWN * m, d), F32),
-            pltpu.VMEM((6, hu, n_tp, d), BF16),
             dma((2,)), dma((n + 1,)), dma((5,)), dma((n + 4, 2)), dma((n + 8,)), dma((5,)), dma((3,)), dma((3,)),
             dma((2,)), dma((2, 2)), dma((2,)), dma((2,)), dma((2,)), dma((2,)), dma(()), dma(()),
-            dma((2,)), dma((2,)), dma((4,)), dma((2,)),
+            dma((2,)), dma((2,)), dma((4,)),
         ],
         compiler_params=pltpu.CompilerParams(
-            collective_id=0, has_side_effects=True, vmem_limit_bytes=67043328
+            collective_id=0, has_side_effects=True, vmem_limit_bytes=46 * 1024 * 1024
         ),
-    )(
-        tokens[0],
-        gain_first[None], gate_first, up_first, down_first,
-        gain_second[None], gate_second, up_second, down_second,
-    )
+    )(*[
+        pltpu.with_memory_space_constraint(a, pltpu.HBM)
+        for a in (
+            tokens[0],
+            gain_first[None], gate_first, up_first, down_first,
+            gain_second[None], gate_second, up_second, down_second,
+        )
+    ]    )
     mixed, *served = pl.pallas_call(
         functools.partial(deliver, 7),
         out_shape=tuple(jax.ShapeDtypeStruct(r.shape, r.dtype) for r in results),
-        in_specs=[hbm] * 7,
+        in_specs=[vmem] * 7,
         out_specs=(hbm,) * 7,
-        scratch_shapes=[pltpu.VMEM(r.shape, r.dtype) for r in results] + [dma((7,)), dma((7,))],
+        scratch_shapes=[dma((7,))],
+        compiler_params=pltpu.CompilerParams(vmem_limit_bytes=1024 * 1024),
     )(*results)
     return (mixed[None],) + tuple(jnp.swapaxes(r, 0, 1) for r in served)
 

time: 79.7 us -> 78 us (0.979)
  Pallas kernels: 78.9 us -> 77.2 us
    pallas_call x1, Pallas kernels: 2.45 us -> 1.4 us  [shards(): pl.pallas_call(functools.partial(deliver, 7), out_shape=tuple((jax.ShapeD...]
where the time goes in v7:
time: 78 us; the launch traced here: 77.8 us
  Pallas kernels  77.2 us (99%)
    pallas_call x1, Pallas kernels, shards(): pl.pallas_call(functools.partial(kernel, n, n_tp, hu, fd), out_shape=(jax...  75.8 us

profile of v7, /device:TPU:1, one launch (start us, length us, event | category | flops | bytes accessed | tf_op | source)
XLA Modules:
  0.0 77.8 jit_solution(1023010390610801396)
XLA Ops:
  0.6 75.8 %shard_map.144 = (bf16[4,2048]{1,0:T(4,128)(2,1)S(1)}, bf16[11,8,2048]{2,1,0:T(8,128)(2,1)S(1)}, bf16[11,8,2048]{2,1,0:T(8,128)(2,1)S(1)}, bf16[11,8,2048]{2,1,0...) custom-call(bf16[256,2048]{1,0:T(8,128)(2,1)} %bitcast.10, ...), custom_call_target="tpu_custom_call" | custom-call | tf_op jit(solution)/shard_map/pallas_call | solution.py:464
  76.4 1.4 %shard_map.145 = (bf16[4,2048]{1,0:T(4,128)(2,1)}, bf16[11,8,2048]{2,1,0:T(8,128)(2,1)}, bf16[11,8,2048]{2,1,0:T(8,128)(2,1)}, bf16[11,8,2048]{2,1,0:T(8,128)(2,...) custom-call(bf16[4,2048]{1,0:T(4,128)(2,1)S(1)} %get-tuple-element.21.refs_0_, ...), custom_call_target="tpu_custom_call" | custom-call | tf_op jit(solution)/shard_map/pallas_call | solution.py:511

commit v8 on v7

--- a/solution.py
+++ b/solution.py
@@ -10,6 +10,7 @@
 MESH = pl.DeviceIdType.MESH
 F32, BF16 = jnp.float32, jnp.bfloat16
 SENT = 12
+EARLY = 2
 OWN = 4
 
 
@@ -27,9 +28,9 @@
     tokens_hbm, gain_one, gate_one, up_one, down_one, gain_two, gate_two, up_two, down_two,
     mixed, out_0, out_1, out_2, out_3, out_4, out_5,
     tokens, gains, trained, stack, turned, outgoing, incoming, placing, weights_8, weights_4, ready, normed,
-    part, landed, group, line, gathered, part_two, landed_two, group_two, owner_two, middle, residual,
+    part, landed, group, line, gathered, part_two, landed_two, middle, residual,
     w_send, w_recv, x_send, near_recv, half_recv, die_recv, quad_send, quad_recv, r_send, r_recv,
-    l_send, l_recv, two_send, two_recv, q_send, q_recv, g_send, g_recv, in_sem,
+    l_send, l_recv, two_send, two_recv, g_send, g_recv, in_sem,
 ):
     staged = (out_0, out_1, out_2, out_3, out_4, out_5)
     fs = n * n
@@ -80,7 +81,8 @@
         pl.semaphore_signal(barrier, inc=1, device_id=(lax.rem(f + k, fs), t), device_id_type=MESH)
 
     around = {1: (), 2: (1,), 4: (1, -1)}[nx]
-    for step in around:
+    across = (2,) if nx == 4 else ()
+    for step in around + across:
         pl.semaphore_signal(barrier, inc=1, device_id=along(step), device_id_type=MESH)
     pl.semaphore_signal(barrier, inc=1, device_id=partner, device_id_type=MESH)
 
@@ -108,7 +110,7 @@
         chosen = (inner // 32 == i) & (lane_in == lane_out // 128 * 32 + inner % 32)
         placing[i] = jnp.where(chosen, 1.0, 0.0).astype(BF16)
 
-    pl.semaphore_wait(barrier, fs - 1 + len(around) + 1)
+    pl.semaphore_wait(barrier, fs - 1 + len(around + across) + 1)
 
     offsets = [(dz, dy) for dz in range(n) for dy in range(n) if dz or dy]
     offsets.sort(key=lambda o: (min(o[0], n - o[0]), -min(o[1], n - o[1])))
@@ -195,6 +197,8 @@
         columns = pl.ds(columns_of(u), strip)
         for h, step in enumerate(around):
             send_piece(0, t, x_send.at[0], near_recv.at[u, h], along(step), columns)
+        for step in across if u >= n // 2 else ():
+            send_piece(0, t, x_send.at[0], half_recv.at[u], along(step), columns)
         send_piece(0, t, x_send.at[0], die_recv.at[0], partner, columns)
 
     def stream_relay(u):
@@ -202,7 +206,7 @@
         for h, step in enumerate(around):
             slot = slot_of(-step, c)
             taken(near_recv.at[u, h], strip)
-            if nx == 4 and h == u % 2:
+            if nx == 4 and h == u % 2 and u < n // 2:
                 send_piece(0, slot, x_send.at[0], half_recv.at[u], along(step), columns)
             send_piece(0, slot, x_send.at[0], die_recv.at[0], partner, columns)
 
@@ -266,54 +270,29 @@
     def branch_of(hidden, down):
         return jnp.dot(hidden, down, preferred_element_type=F32).astype(BF16)
 
-    def send_blocks(source, target, me, count, send, recv, device):
-        for k in far_first(count):
-            peer = lax.rem(me + k, count)
-            remote(source.at[peer], target.at[me], send, recv, device(peer)).start()
-
-        pltpu.make_async_copy(source.at[me], target.at[me], recv).start()
-
-    def reduced(target, count, recv):
-        drain(target, recv)
-        total = target[0].astype(F32)
-        for k in range(1, count):
-            total = total + target[k].astype(F32)
-        return total
-
-    def hand_groups(total, held, targets, me, own, send, recv, device):
-        for k, peer in enumerate(targets):
-            held[k] = total[k * OWN : (k + 1) * OWN].astype(BF16)
-
-            @pl.when(peer != me)
-            def _():
-                remote(held.at[k], own.at[me], send, recv, device(peer)).start()
-
-            @pl.when(peer == me)
-            def _():
-                pltpu.make_async_copy(held.at[k], own.at[me], recv).start()
-
     def added(own, count):
         total = own[0].astype(F32)
         for k in range(1, count):
             total = total + own[k].astype(F32)
         return total
 
-    for u in range(n + 6):
+    quad = [((z + 1 - 2 * ez) * n + y, t), (z * n + y + 1 - 2 * ey, t)]
+    quad.append(((z + 1 - 2 * ez) * n + y + 1 - 2 * ey, t))
+    for u in range(n + 4):
+        if u == n + EARLY:
+            drain(incoming.at[1], w_recv.at[n])
+            merge(1, 0, fs // 4, 0)
+            for k, device in enumerate(quad):
+                for held in (weights_8, weights_4):
+                    remote(
+                        held.at[1, t], held.at[2 + k, t], quad_send.at[k], quad_recv.at[k], device
+                    ).start()
         if u < n:
             stream(u)
         if 3 <= u < n + 3:
             stream_relay(u - 3)
         if 6 <= u:
-            if u == n + 4:
-                break
             stream_finish(u - 6)
-    drain(incoming.at[1], w_recv.at[n])
-    merge(1, 0, fs // 4, 0)
-    quad = [((z + 1 - 2 * ez) * n + y, t), (z * n + y + 1 - 2 * ey, t)]
-    quad.append(((z + 1 - 2 * ez) * n + y + 1 - 2 * ey, t))
-    for k, device in enumerate(quad):
-        for held in (weights_8, weights_4):
-            remote(held.at[1, t], held.at[2 + k, t], quad_send.at[k], quad_recv.at[k], device).start()
     spread(1)
     stream_finish(n - 2)
     stream_finish(n - 1)
@@ -372,9 +351,12 @@
     sum_cut(0)
     relay(2)
     sum_cut(1)
+    relay(3)
+    relay(4)
     finish(1)
-    relay(3)
     prepare(1)
+    finish(2)
+    prepare(2)
     own_slot = jnp.where(even, q // 2, m // 2 + p // 2)
     for side in range(2):
         drain(line.at[side], l_recv.at[side])
@@ -392,9 +374,6 @@
                 gathered.at[side, me], gathered.at[side, me], g_send.at[side], g_recv.at[side],
                 at_two(peer, q) if side == 0 else at_two(p, peer),
             ).start()
-    finish(2)
-    relay(4)
-    prepare(2)
     finish(3)
     prepare(3)
     finish(4)
@@ -403,25 +382,24 @@
     for side in range(2):
         drain(gathered.at[side, pl.ds(0, m - 1)], g_recv.at[side])
     hidden = hidden_of(gathered[...].reshape(2 * quarter, d), ready[0], ready[1])
-    branch = branch_of(hidden, ready[2])
-    part_two[...] = branch.reshape(part_two.shape)
-    for side in range(2):
-        send_blocks(
-            part_two.at[side], landed_two.at[side], p if side == 0 else q, m, two_send.at[side],
-            two_recv.at[side],
-            (lambda peer: at_two(peer, q)) if side == 0 else (lambda peer: at_two(p, peer)),
+    branch = jnp.dot(hidden, ready[2], preferred_element_type=F32)
+    for k in range(m * m):
+        part_two[k] = branch[k * OWN : (k + 1) * OWN].astype(BF16)
+
+    def place_of(pp, qq):
+        return jnp.where(
+            lax.rem(pp + qq, 2) == 0, pp * (m // 2) + qq // 2, m * m // 2 + qq * (m // 2) + pp // 2
         )
+
+    hops = [(dp, dq) for dp in range(m) for dq in range(m) if dp or dq]
+    hops.sort(key=lambda o: -(min(o[0], m - o[0]) + min(o[1], m - o[1])))
+    for dp, dq in hops:
+        pp, qq = lax.rem(p + dp, m), lax.rem(q + dq, m)
+        remote(
+            part_two.at[place_of(pp, qq)], landed_two.at[p * m + q], two_send, two_recv, at_two(pp, qq)
+        ).start()
+    pltpu.make_async_copy(part_two.at[place_of(p, q)], landed_two.at[p * m + q], two_recv).start()
     publish(1)
-    total = reduced(landed_two.at[0], m, two_recv.at[0])
-    hand_groups(
-        total, group_two.at[0], [2 * k + lax.rem(p, 2) for k in range(m // 2)], q,
-        owner_two, q_send, q_recv, lambda peer: at_two(p, peer),
-    )
-    total = reduced(landed_two.at[1], m, two_recv.at[1])
-    hand_groups(
-        total, group_two.at[1], [2 * k + lax.rem(q + 1, 2) for k in range(m // 2)], p,
-        owner_two, q_send, q_recv, lambda peer: at_two(peer, q),
-    )
     for k in range(3):
         taken(quad_send.at[k])
     for s in range(5):
@@ -431,10 +409,9 @@
         drain(part.at[b, pl.ds(0, n - 1)], r_send.at[b])
         drain(line.at[b, pl.ds(0, n - 1)], l_send.at[b])
         drain(gathered.at[b, pl.ds(0, m - 1)], g_send.at[b])
-        drain(gathered.at[b, pl.ds(0, m - 1)], two_send.at[b])
-    drain(owner_two.at[pl.ds(0, m - 1)], q_send)
-    drain(owner_two, q_recv)
-    mixed[...] = (middle[own_slot].astype(F32) + 0.5 * added(owner_two, m)).astype(BF16)
+    drain(part_two.at[pl.ds(0, m * m - 1)], two_send)
+    drain(landed_two, two_recv)
+    mixed[...] = (middle[own_slot].astype(F32) + 0.5 * added(landed_two, m * m)).astype(BF16)
 
 
 def deliver(count, *refs):
@@ -487,14 +464,12 @@
             pltpu.VMEM((2, 2, OWN * m // 2, d), BF16),
             pltpu.VMEM((2, n, OWN * m // 2, d), BF16),
             pltpu.VMEM(two, BF16),
-            pltpu.VMEM(two, BF16),
-            pltpu.VMEM(two, BF16),
-            pltpu.VMEM((2, m // 2, OWN, d), BF16),
-            pltpu.VMEM((m, OWN, d), BF16),
+            pltpu.VMEM((m * m, OWN, d), BF16),
+            pltpu.VMEM((m * m, OWN, d), BF16),
             pltpu.VMEM((m, OWN, d), BF16),
             pltpu.VMEM((OWN * m, d), F32),
             dma((2,)), dma((n + 1,)), dma((5,)), dma((n + 4, 2)), dma((n + 8,)), dma((5,)), dma((3,)), dma((3,)),
-            dma((2,)), dma((2, 2)), dma((2,)), dma((2,)), dma((2,)), dma((2,)), dma(()), dma(()),
+            dma((2,)), dma((2, 2)), dma((2,)), dma((2,)), dma(()), dma(()),
             dma((2,)), dma((2,)), dma((4,)),
         ],
         compiler_params=pltpu.CompilerParams(

time: 78 us -> 74.7 us (0.958)
  Pallas kernels: 77.2 us -> 73.9 us
    pallas_call x1, Pallas kernels: 75.8 us -> 72.5 us  [shards(): pl.pallas_call(functools.partial(kernel, n, n_tp, hu, fd), out_shape=(jax...]
where the time goes in v8:
time: 74.7 us; the launch traced here: 74.5 us
  Pallas kernels  73.9 us (99%)
    pallas_call x1, Pallas kernels, shards(): pl.pallas_call(functools.partial(kernel, n, n_tp, hu, fd), out_shape=(jax...  72.5 us

profile of v8, /device:TPU:1, one launch (start us, length us, event | category | flops | bytes accessed | tf_op | source)
XLA Modules:
  0.0 74.5 jit_solution(5250361273976258241)
XLA Ops:
  0.6 72.5 %shard_map.144 = (bf16[4,2048]{1,0:T(4,128)(2,1)S(1)}, bf16[11,8,2048]{2,1,0:T(8,128)(2,1)S(1)}, bf16[11,8,2048]{2,1,0:T(8,128)(2,1)S(1)}, bf16[11,8,2048]{2,1,0...) custom-call(bf16[256,2048]{1,0:T(8,128)(2,1)} %bitcast.10, ...), custom_call_target="tpu_custom_call" | custom-call | tf_op jit(solution)/shard_map/pallas_call | solution.py:441
  73.1 1.4 %shard_map.145 = (bf16[4,2048]{1,0:T(4,128)(2,1)}, bf16[11,8,2048]{2,1,0:T(8,128)(2,1)}, bf16[11,8,2048]{2,1,0:T(8,128)(2,1)}, bf16[11,8,2048]{2,1,0:T(8,128)(2,...) custom-call(bf16[4,2048]{1,0:T(4,128)(2,1)S(1)} %get-tuple-element.21.refs_0_, ...), custom_call_target="tpu_custom_call" | custom-call | tf_op jit(solution)/shard_map/pallas_call | solution.py:486

commit v9 on v8

--- a/solution.py
+++ b/solution.py
@@ -10,7 +10,10 @@
 MESH = pl.DeviceIdType.MESH
 F32, BF16 = jnp.float32, jnp.bfloat16
 SENT = 12
-EARLY = 2
+EARLY = 4
+RELAY = 6
+FINISH = 7
+DIRECT = 0
 OWN = 4
 
 
@@ -76,9 +79,12 @@
 
     barrier = pltpu.get_barrier_semaphore()
 
-    @pl.loop(1, fs)
-    def _(k):
-        pl.semaphore_signal(barrier, inc=1, device_id=(lax.rem(f + k, fs), t), device_id_type=MESH)
+    offsets = [(dz, dy) for dz in range(n) for dy in range(n) if dz or dy]
+    offsets.sort(key=lambda o: -(min(o[0], n - o[0]) + min(o[1], n - o[1])))
+    for dz, dy in offsets:
+        pl.semaphore_signal(
+            barrier, inc=1, device_id=at(lax.rem(z + dz, n), lax.rem(y + dy, n)), device_id_type=MESH
+        )
 
     around = {1: (), 2: (1,), 4: (1, -1)}[nx]
     across = (2,) if nx == 4 else ()
@@ -89,33 +95,22 @@
     hidden_units = gate_one.shape[1]
     stack[...] = jnp.zeros_like(stack)
     drain(gains, in_sem.at[3])
+    ones = jnp.ones((1, fd), F32)
+    live = lax.broadcasted_iota(jnp.int32, (SENT, 128), 0) < hu
+    by_strip = sorted(offsets, key=lambda o: (min(o[0], n - o[0]), -min(o[1], n - o[1])))
     for b in range(2):
         drain(trained.at[b], in_sem.at[b])
         for w in range(3):
             stack[w * fd : (w + 1) * fd, 0:hidden_units] = trained[b, w]
-        ones = jnp.ones((1, fd), F32)
         scale = jnp.concatenate([gains[b], gains[b], ones, ones], axis=1)
         turned[...] = stack[...].T * scale
-        live = lax.broadcasted_iota(jnp.int32, (SENT, 128), 0) < hu
         for k in range(fs):
             rows = jnp.where(live, turned[k * hu : k * hu + SENT, :], 0.0)
             for g in range(SENT // 4):
                 outgoing[b, k, g] = rows[4 * g : 4 * g + 4].astype(BF16)
-
-    lanes = 3 * 128
-    lane_in = lax.broadcasted_iota(jnp.int32, (128, lanes), 0)
-    lane_out = lax.broadcasted_iota(jnp.int32, (128, lanes), 1)
-    inner = lane_out % 128
-    for i in range(4):
-        chosen = (inner // 32 == i) & (lane_in == lane_out // 128 * 32 + inner % 32)
-        placing[i] = jnp.where(chosen, 1.0, 0.0).astype(BF16)
-
-    pl.semaphore_wait(barrier, fs - 1 + len(around + across) + 1)
-
-    offsets = [(dz, dy) for dz in range(n) for dy in range(n) if dz or dy]
-    offsets.sort(key=lambda o: (min(o[0], n - o[0]), -min(o[1], n - o[1])))
-    for b in range(2):
-        for dz, dy in offsets:
+        if b == 0:
+            pl.semaphore_wait(barrier, fs - 1 + len(around + across) + 1)
+        for dz, dy in by_strip if b == 0 else offsets:
             peer = lax.rem(z + dz, n) * n + lax.rem(y + dy, n)
             remote(
                 outgoing.at[b, peer],
@@ -128,6 +123,14 @@
         pltpu.make_async_copy(
             outgoing.at[b, f], incoming.at[b, lax.rem(f, 4), f // 4], w_recv.at[z if b == 0 else n]
         ).start()
+
+    lanes = 3 * 128
+    lane_in = lax.broadcasted_iota(jnp.int32, (128, lanes), 0)
+    lane_out = lax.broadcasted_iota(jnp.int32, (128, lanes), 1)
+    inner = lane_out % 128
+    for i in range(4):
+        chosen = (inner // 32 == i) & (lane_in == lane_out // 128 * 32 + inner % 32)
+        placing[i] = jnp.where(chosen, 1.0, 0.0).astype(BF16)
 
     drain(tokens, in_sem.at[2])
     wide = tokens[...].astype(F32)
@@ -197,7 +200,7 @@
         columns = pl.ds(columns_of(u), strip)
         for h, step in enumerate(around):
             send_piece(0, t, x_send.at[0], near_recv.at[u, h], along(step), columns)
-        for step in across if u >= n // 2 else ():
+        for step in across if u >= DIRECT else ():
             send_piece(0, t, x_send.at[0], half_recv.at[u], along(step), columns)
         send_piece(0, t, x_send.at[0], die_recv.at[0], partner, columns)
 
@@ -206,7 +209,7 @@
         for h, step in enumerate(around):
             slot = slot_of(-step, c)
             taken(near_recv.at[u, h], strip)
-            if nx == 4 and h == u % 2 and u < n // 2:
+            if nx == 4 and h == u % 2 and u < DIRECT:
                 send_piece(0, slot, x_send.at[0], half_recv.at[u], along(step), columns)
             send_piece(0, slot, x_send.at[0], die_recv.at[0], partner, columns)
 
@@ -278,7 +281,7 @@
 
     quad = [((z + 1 - 2 * ez) * n + y, t), (z * n + y + 1 - 2 * ey, t)]
     quad.append(((z + 1 - 2 * ez) * n + y + 1 - 2 * ey, t))
-    for u in range(n + 4):
+    for u in range(n + FINISH):
         if u == n + EARLY:
             drain(incoming.at[1], w_recv.at[n])
             merge(1, 0, fs // 4, 0)
@@ -287,15 +290,13 @@
                     remote(
                         held.at[1, t], held.at[2 + k, t], quad_send.at[k], quad_recv.at[k], device
                     ).start()
+            spread(1)
         if u < n:
             stream(u)
-        if 3 <= u < n + 3:
-            stream_relay(u - 3)
-        if 6 <= u:
-            stream_finish(u - 6)
-    spread(1)
-    stream_finish(n - 2)
-    stream_finish(n - 1)
+        if RELAY <= u < n + RELAY:
+            stream_relay(u - RELAY)
+        if FINISH <= u:
+            stream_finish(u - FINISH)
     collected(0)
     hidden = hidden_of(normed[...], units(0, 0), units(0, 1))
     down_one = units(0, 2)

time: 74.7 us -> 73.1 us (0.979)
  Pallas kernels: 73.9 us -> 72.3 us
    pallas_call x1, Pallas kernels: 72.5 us -> 70.9 us  [shards(): pl.pallas_call(functools.partial(kernel, n, n_tp, hu, fd), out_shape=(jax...]
where the time goes in v9:
time: 73.1 us; the launch traced here: 72.9 us
  Pallas kernels  72.3 us (99%)
    pallas_call x1, Pallas kernels, shards(): pl.pallas_call(functools.partial(kernel, n, n_tp, hu, fd), out_shape=(jax...  70.9 us

profile of v9, /device:TPU:1, one launch (start us, length us, event | category | flops | bytes accessed | tf_op | source)
XLA Modules:
  0.0 72.9 jit_solution(11704613637629132207)
XLA Ops:
  0.6 70.9 %shard_map.144 = (bf16[4,2048]{1,0:T(4,128)(2,1)S(1)}, bf16[11,8,2048]{2,1,0:T(8,128)(2,1)S(1)}, bf16[11,8,2048]{2,1,0:T(8,128)(2,1)S(1)}, bf16[11,8,2048]{2,1,0...) custom-call(bf16[256,2048]{1,0:T(8,128)(2,1)} %bitcast.10, ...), custom_call_target="tpu_custom_call" | custom-call | tf_op jit(solution)/shard_map/pallas_call | solution.py:442
  71.5 1.4 %shard_map.145 = (bf16[4,2048]{1,0:T(4,128)(2,1)}, bf16[11,8,2048]{2,1,0:T(8,128)(2,1)}, bf16[11,8,2048]{2,1,0:T(8,128)(2,1)}, bf16[11,8,2048]{2,1,0:T(8,128)(2,...) custom-call(bf16[4,2048]{1,0:T(4,128)(2,1)S(1)} %get-tuple-element.21.refs_0_, ...), custom_call_target="tpu_custom_call" | custom-call | tf_op jit(solution)/shard_map/pallas_call | solution.py:487

commit v10 on v9

--- a/solution.py
+++ b/solution.py
@@ -10,7 +10,7 @@
 MESH = pl.DeviceIdType.MESH
 F32, BF16 = jnp.float32, jnp.bfloat16
 SENT = 12
-EARLY = 4
+EARLY = 3
 RELAY = 6
 FINISH = 7
 DIRECT = 0
@@ -298,13 +298,16 @@
         if FINISH <= u:
             stream_finish(u - FINISH)
     collected(0)
-    hidden = hidden_of(normed[...], units(0, 0), units(0, 1))
-    down_one = units(0, 2)
+    gate_one_units, up_one_units, down_one = units(0, 0), units(0, 1), units(0, 2)
+    hidden = [None, None]
     wide = d // 2
     for cut in range(2):
         columns = slice(cut * wide, (cut + 1) * wide)
         for side in range(2):
-            branch = branch_of(hidden[side * half : (side + 1) * half], down_one[:, columns])
+            if cut == 0:
+                rows = normed[side * half : (side + 1) * half, :]
+                hidden[side] = hidden_of(rows, gate_one_units, up_one_units)
+            branch = branch_of(hidden[side], down_one[:, columns])
             part[side, :, :, columns] = branch.reshape(n, block, wide)
             me = z if side == 0 else y
             for k in far_first(n):

time: 73.1 us -> 72.8 us (level); the launches traced: 72.9 us -> 71.6 us
  Pallas kernels: 72.3 us -> 70.9 us
    pallas_call x1, Pallas kernels: 70.9 us -> 69.5 us  [shards(): pl.pallas_call(functools.partial(kernel, n, n_tp, hu, fd), out_shape=(jax...]
where the time goes in v10:
time: 72.8 us; the launch traced here: 71.6 us
  Pallas kernels  70.9 us (97%)
    pallas_call x1, Pallas kernels, shards(): pl.pallas_call(functools.partial(kernel, n, n_tp, hu, fd), out_shape=(jax...  69.5 us

profile of v10, /device:TPU:1, one launch (start us, length us, event | category | flops | bytes accessed | tf_op | source)
XLA Modules:
  0.0 71.6 jit_solution(14839764850740912292)
XLA Ops:
  0.6 69.5 %shard_map.144 = (bf16[4,2048]{1,0:T(4,128)(2,1)S(1)}, bf16[11,8,2048]{2,1,0:T(8,128)(2,1)S(1)}, bf16[11,8,2048]{2,1,0:T(8,128)(2,1)S(1)}, bf16[11,8,2048]{2,1,0...) custom-call(bf16[256,2048]{1,0:T(8,128)(2,1)} %bitcast.10, ...), custom_call_target="tpu_custom_call" | custom-call | tf_op jit(solution)/shard_map/pallas_call | solution.py:445
  70.2 1.4 %shard_map.145 = (bf16[4,2048]{1,0:T(4,128)(2,1)}, bf16[11,8,2048]{2,1,0:T(8,128)(2,1)}, bf16[11,8,2048]{2,1,0:T(8,128)(2,1)}, bf16[11,8,2048]{2,1,0:T(8,128)(2,...) custom-call(bf16[4,2048]{1,0:T(4,128)(2,1)S(1)} %get-tuple-element.21.refs_0_, ...), custom_call_target="tpu_custom_call" | custom-call | tf_op jit(solution)/shard_map/pallas_call | solution.py:490
